TPU v7x, 32 devices: a whole 2x2x4 slice. The times are simulated.
32 devices in a mesh: grp: 2 (over y), fs: 4 (over z), tp: 4 (over x, core).
Axes of the slice: x: 2, y: 2, z: 4, core: 2. Of those that a mesh axis runs over, the one named last changes fastest.
Arguments:
- tokens: bfloat16 [8192, 2048], P(('grp', 'fs'), 'tp'), parts along dimension 0, may hold values from -6 to 6
- mixer_gain: float32 [2048], replicated, may hold values from 0.1 to 1.9
- branch_weight: float32 [2048, 1024], P('fs', 'tp'), may hold values from -0.125 to 0.125
- gelu_weight: float32 [2048, 1024], P('fs', 'tp'), may hold values from -0.125 to 0.125
- branch_scale: float32 [4, 256], P('fs', 'tp'), may hold values from 0.5 to 2
- gelu_scale: float32 [4, 256], P('fs', 'tp'), may hold values from 0.5 to 2
- branch_taps: float32 [4, 1024], P(None, 'tp'), may hold values from -3 to 3
- recur_gate: bfloat16 [16, 64, 64], P('tp'), may hold values from -0.75 to 0.75
- input_gate: bfloat16 [16, 64, 64], P('tp'), may hold values from -0.75 to 0.75
- decay_param: float32 [1024], P('tp'), may hold values from 4 to 7
- out_weight: float32 [1024, 2048], P('tp', 'fs'), may hold values from -0.5 to 0.5
- out_scale: float32 [4, 512], P('fs'), may hold values from 0.5 to 2
- ffn_gain: float32 [2048], replicated, may hold values from 0.1 to 1.9
- upgate_weight: float32 [2048, 5632], P('fs', 'tp'), may hold values from -0.125 to 0.125
- upval_weight: float32 [2048, 5632], P('fs', 'tp'), may hold values from -0.125 to 0.125
- upgate_scale: float32 [4, 1408], P('fs', 'tp'), may hold values from 0.5 to 2
- upval_scale: float32 [4, 1408], P('fs', 'tp'), may hold values from 0.5 to 2
- upgate_taps: float32 [3, 5632], P(None, 'tp'), may hold values from -3 to 3
- upval_taps: float32 [3, 5632], P(None, 'tp'), may hold values from -3 to 3
- down_weight: float32 [5632, 2048], P('tp', 'fs'), may hold values from -0.15625 to 0.15625
- down_scale: float32 [4, 512], P('fs'), may hold values from 0.5 to 2
Outputs:
- layer_out: bfloat16 [8192, 2048], P(('grp', 'fs'), 'tp'), parts along dimension 0
There are 2 independent parts, one for each index of `grp`. A program takes and returns all parts, laid end to end along the dimension named above; an argument that names none is the same for every part. Nothing has to cross between parts.
All inputs are finite; a program needn't handle non-finite values.
Results may differ from a plain program's by a relative error of at most 0.024.
Values may be sent and summed in bfloat16 or wider, within the bound.
A program may use at most 128 MiB of HBM per device.

v0:
```python
import jax
import jax.numpy as jnp
from jax import lax
from jax.sharding import PartitionSpec as P

SEQ_LEN = 512


def rms_rows(values_in, norm_gain):
    values = values_in.astype(jnp.float32)
    inverse = lax.rsqrt(jnp.mean(values * values, axis=-1, keepdims=True) + 1e-06)
    return (values * inverse * norm_gain).astype(jnp.bfloat16)


def expand_scale(gathered):
    return gathered.T.reshape(-1)


def causal_mix(values, filter_taps, seq_len):
    columns = values.shape[-1]
    grouped = values.reshape(-1, seq_len, columns)
    tap_count = filter_taps.shape[0]
    padded = jnp.pad(grouped, ((0, 0), (tap_count - 1, 0), (0, 0)))
    totals = padded[:, 0:seq_len] * filter_taps[0]
    for k in range(1, tap_count):
        totals = totals + padded[:, k : k + seq_len] * filter_taps[k]
    return totals.reshape(-1, columns)


def combine_pairs(earlier, later):
    return (earlier[0] * later[0], later[0] * earlier[1] + later[1])


def run_scan(factors, inputs, seq_len):
    columns = factors.shape[-1]
    pair = (factors.reshape(-1, seq_len, columns), inputs.reshape(-1, seq_len, columns))
    _, states = lax.associative_scan(combine_pairs, pair, axis=1)
    return states.reshape(-1, columns)


def add_rows(left, weight_piece):
    return jnp.dot(left, weight_piece, preferred_element_type=jnp.float32)


def per_device(
    tokens,
    mixer_gain,
    branch_weight,
    gelu_weight,
    branch_scale,
    gelu_scale,
    branch_taps,
    recur_gate,
    input_gate,
    decay_param,
    out_weight,
    out_scale,
    ffn_gain,
    upgate_weight,
    upval_weight,
    upgate_scale,
    upval_scale,
    upgate_taps,
    upval_taps,
    down_weight,
    down_scale,
):
    mixer_scales = (
        lax.all_gather(branch_scale, "fs", axis=0, tiled=True),
        lax.all_gather(gelu_scale, "fs", axis=0, tiled=True),
        lax.all_gather(out_scale, "fs", axis=0, tiled=True),
    )
    gathered = lax.all_gather(tokens, "tp", axis=1, tiled=True)
    normed = rms_rows(gathered, mixer_gain)
    branch = add_rows(
        normed, lax.all_gather(branch_weight.astype(jnp.bfloat16), "fs", axis=0, tiled=True)
    )
    gelu_in = add_rows(
        normed, lax.all_gather(gelu_weight.astype(jnp.bfloat16), "fs", axis=0, tiled=True)
    )
    branch = branch * expand_scale(mixer_scales[0])
    gelu_in = gelu_in * expand_scale(mixer_scales[1])
    convolved = causal_mix(branch, branch_taps, SEQ_LEN).astype(jnp.bfloat16)
    local_blocks = recur_gate.shape[0]
    blocks = convolved.reshape(convolved.shape[0], local_blocks, recur_gate.shape[1])
    channels = convolved.shape[1]
    recur = jax.nn.sigmoid(
        jnp.einsum("rnc,ncd->rnd", blocks, recur_gate, preferred_element_type=jnp.float32).reshape(
            -1, channels
        )
    )
    input_rate = jax.nn.sigmoid(
        jnp.einsum("rnc,ncd->rnd", blocks, input_gate, preferred_element_type=jnp.float32).reshape(
            -1, channels
        )
    )
    log_decay = -8.0 * recur * jax.nn.softplus(-decay_param)
    decay_rate = jnp.exp(log_decay)
    driven = jnp.sqrt(-jnp.expm1(2.0 * log_decay)) * input_rate * convolved.astype(jnp.float32)
    states = run_scan(decay_rate, driven, SEQ_LEN)
    gated_state = (states * jax.nn.gelu(gelu_in)).astype(jnp.bfloat16)
    out_cols = expand_scale(mixer_scales[2])
    tp_count = lax.axis_size("tp")
    feature_width = tokens.shape[1]
    whole_state = lax.all_gather(gated_state, "tp", axis=1, tiled=True)
    row_block = lax.all_gather(out_weight.astype(jnp.bfloat16), "fs", axis=1, tiled=True)
    own_columns = lax.all_to_all(row_block, "tp", split_axis=1, concat_axis=0, tiled=True)
    first_feature = lax.axis_index("tp") * feature_width
    own_scales = lax.dynamic_slice_in_dim(out_cols, first_feature, feature_width, 0)
    block_rows = whole_state.shape[1] // tp_count
    mixer_sum = jnp.zeros((whole_state.shape[0], feature_width), jnp.float32)
    for index in range(tp_count):
        partial_value = (
            jnp.dot(
                whole_state[:, index * block_rows : (index + 1) * block_rows],
                own_columns[index * block_rows : (index + 1) * block_rows],
                preferred_element_type=jnp.float32,
            )
            * own_scales
        )
        mixer_sum = mixer_sum + partial_value.astype(jnp.bfloat16).astype(jnp.float32)
    hidden_state = (tokens.astype(jnp.float32) + mixer_sum).astype(jnp.bfloat16)
    ffn_scales = (
        lax.all_gather(upgate_scale, "fs", axis=0, tiled=True),
        lax.all_gather(upval_scale, "fs", axis=0, tiled=True),
        lax.all_gather(down_scale, "fs", axis=0, tiled=True),
    )
    gathered_ffn = lax.all_gather(hidden_state, "tp", axis=1, tiled=True)
    normed_ffn = rms_rows(gathered_ffn, ffn_gain)
    upgate_bf = upgate_weight.astype(jnp.bfloat16)
    upval_bf = upval_weight.astype(jnp.bfloat16)
    gate_full, value_full = (
        lax.all_gather(upgate_bf, "fs", axis=0, tiled=True),
        lax.all_gather(upval_bf, "fs", axis=0, tiled=True),
    )
    up_gate = jnp.dot(normed_ffn, gate_full, preferred_element_type=jnp.float32)
    up_val = jnp.dot(normed_ffn, value_full, preferred_element_type=jnp.float32)
    up_gate = up_gate * expand_scale(ffn_scales[0])
    up_val = up_val * expand_scale(ffn_scales[1])
    conv_gate = causal_mix(up_gate, upgate_taps, SEQ_LEN)
    conv_val = causal_mix(up_val, upval_taps, SEQ_LEN)
    ffn_hidden = (jax.nn.silu(conv_gate) * conv_val).astype(jnp.bfloat16)
    down_cols = expand_scale(ffn_scales[2])
    ffn_terms = (
        jnp.dot(
            ffn_hidden,
            lax.all_gather(down_weight.astype(jnp.bfloat16), "fs", axis=1, tiled=True),
            preferred_element_type=jnp.float32,
        )
        * down_cols
    ).astype(jnp.bfloat16)
    ffn_sum = lax.psum_scatter(ffn_terms, "tp", scatter_dimension=1, tiled=True).astype(jnp.float32)
    return (hidden_state.astype(jnp.float32) + ffn_sum).astype(jnp.bfloat16)


def solution(mesh):
    in_specs = (
        P(("grp", "fs"), "tp"),
        P(),
        P("fs", "tp"),
        P("fs", "tp"),
        P("fs", "tp"),
        P("fs", "tp"),
        P(None, "tp"),
        P("tp", None, None),
        P("tp", None, None),
        P("tp"),
        P("tp", "fs"),
        P("fs", None),
        P(),
        P("fs", "tp"),
        P("fs", "tp"),
        P("fs", "tp"),
        P("fs", "tp"),
        P(None, "tp"),
        P(None, "tp"),
        P("tp", "fs"),
        P("fs", None),
    )
    out_specs = P(("grp", "fs"), "tp")
    return jax.shard_map(
        per_device, mesh=mesh, in_specs=in_specs, out_specs=out_specs, check_vma=False
    )
```

profile of v0, /device:TPU:0, one launch (start us, length us, event | category | flops | bytes accessed | tf_op | source)
XLA Modules:
  0.0 646.5 jit_solution(5973349437280112789)
XLA Ops:
  7.3 1.8 convert_element_type.98
  9.2 1.8 convert_element_type.102
  11.0 1.9 copy.57
  13.0 12.8 %all-gather = f32[4,1,64]{2,1,0:T(1,128)S(1)} all-gather(f32[1,1,64]{2,1,0:T(1,128)} %bitcast.139), channel_id=1, replica_groups=mesh['grp'=2,'fs'=4,'tp'=4] {'fs'}, dimensions={0}, use_global_device_ids=true | all-gather | bytes 1280 | tf_op jit(solution)/shard_map/all_gather | solution.py:69
  27.5 7.8 %all-gather.1 = f32[4,1,64]{2,1,0:T(1,128)S(1)} all-gather(f32[1,1,64]{2,1,0:T(1,128)} %bitcast.140), channel_id=1, replica_groups=mesh['grp'=2,'fs'=4,'tp'=4] {'fs'}, dimensions={0}, use_global_device_ids=true | all-gather | bytes 1280 | tf_op jit(solution)/shard_map/all_gather | solution.py:70
  36.1 10.0 %all-gather.16.cloned.1.call-done = bf16[1024,2048]{1,0:T(8,128)(2,1)} async-done(((bf16[1024,512]{1,0:T(8,128)(2,1)}), bf16[1024,2048]{1,0:T(8,128)(2,1)}) %all-gather.16.cloned.1.call-update) | async-done | bytes 4194320 | tf_op jit(solution)/shard_map/all_gather | solution.py:73
  46.1 3.1 fusion
  49.2 26.5 %all-gather.18.cloned.1.call-done = bf16[2048,256]{1,0:T(8,128)(2,1)} async-done(((bf16[512,256]{1,0:T(8,128)(2,1)}), bf16[2048,256]{1,0:T(8,128)(2,1)}) %all-gather.18.cloned.1.call-update) | async-done | bytes 1048592 | tf_op jit(solution)/shard_map/all_gather | solution.py:76
  75.7 3.8 convolution_multiply_fusion.3
  83.3 1.4 copy.53
  84.7 1.5 fusion.17
  87.1 1.4 copy.55
  88.5 2.7 multiply_exponential_fusion
  91.3 2.2 slice.307
  93.4 2.2 slice.308
  95.6 2.1 slice.306
  97.7 2.2 slice.310
  99.9 1.7 fusion.53
  104.7 2.0 fusion.54
  108.0 1.6 slice.318
  109.6 1.6 slice.322
  111.2 1.9 fusion.55
  113.1 1.5 slice.325
  114.6 1.5 slice.326
  116.2 1.5 slice.324
  117.7 1.5 slice.328
  122.6 1.4 fusion.57
  124.1 1.4 slice.337
  125.4 1.4 slice.338
  126.8 1.4 slice.336
  128.1 1.4 slice.340
  129.5 1.4 fusion.58
  142.7 1.4 fusion.59
  147.9 1.4 slice.360
  152.3 1.5 slice.323
  153.9 1.5 slice.364
  156.7 1.6 slice.317
  171.0 2.1 pad.78
  173.1 1.8 fusion.44
  174.9 1.6 add.236
  184.9 4.8 fusion.34
  189.7 3.5 all-to-all-start
  193.3 12.2 %all-gather.2 = f32[4,1,512]{2,1,0:T(1,128)S(1)} all-gather(f32[1,1,512]{2,1,0:T(1,128)S(1)} %bitcast.135), channel_id=1, replica_groups=mesh['grp'=2,'fs'=4,'tp'=4] {'fs'}, dimensions={0}, use_global_device_ids=true | all-gather | bytes 10240 | tf_op jit(solution)/shard_map/all_gather | solution.py:71
  205.9 11.0 %all-to-all-done = bf16[256,4,512]{0,2,1:T(8,128)(2,1)S(1)} async-done(((bf16[256,4,512]{0,2,1:T(8,128)(2,1)}), bf16[256,4,512]{0,2,1:T(8,128)(2,1)S(1)}, u32[]{:S(2)}, u32[]{:S(2)}) %all-to-all-start) | async-done | bytes 1048608 | tf_op jit(solution)/shard_map/all_to_all | solution.py:107
  216.9 3.8 all-gather.22.cloned.1.call-done
  220.7 1.5 multiply_convert_fusion.2
  222.2 1.7 multiply_convert_fusion.3
  224.0 1.6 multiply_convert_fusion.1
  225.6 3.4 add_convert_fusion.1
  230.5 3.3 convert_element_type.118
  235.2 11.9 %all-gather.3 = f32[4,1,352]{2,1,0:T(1,128)S(1)} all-gather(f32[1,1,352]{2,1,0:T(1,128)S(1)} %bitcast.137), channel_id=1, replica_groups=mesh['grp'=2,'fs'=4,'tp'=4] {'fs'}, dimensions={0}, use_global_device_ids=true | all-gather | bytes 7040 | tf_op jit(solution)/shard_map/all_gather | solution.py:124
  247.4 11.9 %all-gather.4 = f32[4,1,352]{2,1,0:T(1,128)S(1)} all-gather(f32[1,1,352]{2,1,0:T(1,128)S(1)} %bitcast.138), channel_id=1, replica_groups=mesh['grp'=2,'fs'=4,'tp'=4] {'fs'}, dimensions={0}, use_global_device_ids=true | all-gather | bytes 7040 | tf_op jit(solution)/shard_map/all_gather | solution.py:125
  259.7 11.9 %all-gather.5 = f32[4,1,512]{2,1,0:T(1,128)S(1)} all-gather(f32[1,1,512]{2,1,0:T(1,128)S(1)} %bitcast.136), channel_id=1, replica_groups=mesh['grp'=2,'fs'=4,'tp'=4] {'fs'}, dimensions={0}, use_global_device_ids=true | all-gather | bytes 10240 | tf_op jit(solution)/shard_map/all_gather | solution.py:126
  272.1 3.4 fusion.3
  275.5 94.8 %all-gather.28.cloned.1.call-done = bf16[2048,1408]{1,0:T(8,128)(2,1)} async-done(((bf16[512,1408]{1,0:T(8,128)(2,1)}), bf16[2048,1408]{1,0:T(8,128)(2,1)}) %all-gather.28.cloned.1.call-update) | async-done | bytes 5767184 | tf_op jit(solution)/shard_map/all_gather | solution.py:133
  370.3 12.0 %convolution_multiply_fusion.1 = f32[1024,1408]{1,0:T(8,128)} fusion(bf16[2048,1408]{1,0:T(8,128)(2,1)} %all-gather.28.cloned.1.call-done, f32[1408]{0:T(1024)S(1)} %mul.429, bf16[1024,2048]{1,0:T(8,128)(2,1)} %all-gather.26.cloned.1.call-done, f32[2048]{0:T(1024)S(1)} %copy-done.19, f32[1024]{0:T(1024)S(1)} %add_rsqrt_fusion), kind=kOutput, calls=%fused_computation.21 | convolution fusion | flops 5915410432 | bytes 15746560 | tf_op jit(solution)/shard_map/dot_general | solution.py:136
  382.3 94.6 %all-gather.30.cloned.1.call-done = bf16[2048,1408]{1,0:T(8,128)(2,1)} async-done(((bf16[512,1408]{1,0:T(8,128)(2,1)}), bf16[2048,1408]{1,0:T(8,128)(2,1)}) %all-gather.30.cloned.1.call-update) | async-done | bytes 5767184 | tf_op jit(solution)/shard_map/all_gather | solution.py:134
  476.8 11.9 %convolution_multiply_fusion = f32[1024,1408]{1,0:T(8,128)} fusion(bf16[2048,1408]{1,0:T(8,128)(2,1)} %all-gather.30.cloned.1.call-done, f32[1408]{0:T(1024)S(1)} %mul.442, bf16[1024,2048]{1,0:T(8,128)(2,1)} %all-gather.26.cloned.1.call-done, f32[2048]{0:T(1024)S(1)} %copy-done.19, f32[1024]{0:T(1024)S(1)} %add_rsqrt_fusion), kind=kOutput, calls=%fused_computation.20 | convolution fusion | flops 5915410432 | bytes 15746560 | tf_op jit(solution)/shard_map/dot_general | solution.py:137
  488.7 16.0 %multiply_add_fusion = (f32[2,512,1408]{2,1,0:T(8,128)S(1)}, f32[2,512,1408]{2,1,0:T(8,128)}) fusion(f32[2,512,1408]{2,1,0:T(8,128)} %bitcast.102, f32[1408]{0:T(1024)S(1)} %get-tuple-element.9, f32[1408]{0:T(1024)S(1)} %get-tuple-element.10, f32[1408]{0:T(1024)S(1)} %get-tuple-element.8, f32[2,512,1408]{2,1,0:T(8,128)} %bitcast.101, ...), kind=kLoop, calls=%fused_computation.18 | loop fusion | flops 14417920 | bytes 23102464 | tf_op jit(solution)/shard_map/add | solution.py:26
  504.8 6.6 %fusion.6 = bf16[1024,1408]{1,0:T(8,128)(2,1)} fusion(f32[2,512,1408]{2,1,0:T(8,128)S(1)} %get-tuple-element.35, f32[2,512,1408]{2,1,0:T(8,128)} %get-tuple-element.36), kind=kLoop, calls=%fused_computation.12 | loop fusion | flops 8650752 | bytes 14417920 | tf_op jit(solution)/shard_map/convert_element_type | solution.py:142
  511.3 72.1 %all-gather.32.cloned.1.call-done = bf16[1408,2048]{1,0:T(8,128)(2,1)} async-done(((bf16[1408,512]{1,0:T(8,128)(2,1)}), bf16[1408,2048]{1,0:T(8,128)(2,1)}) %all-gather.32.cloned.1.call-update) | async-done | bytes 5767184 | tf_op jit(solution)/shard_map/all_gather | solution.py:147
  583.4 11.0 %multiply_convert_fusion = bf16[1024,2048]{1,0:T(8,128)(2,1)} fusion(bf16[1024,1408]{1,0:T(8,128)(2,1)} %fusion.6, bf16[1408,2048]{1,0:T(8,128)(2,1)} %all-gather.32.cloned.1.call-done, f32[2048]{0:T(1024)S(1)} %mul.455), kind=kOutput, calls=%fused_computation.10 | convolution fusion | flops 5909774336 | bytes 12853248 | tf_op jit(solution)/shard_map/dot_general | solution.py:145
  594.4 42.8 %reduce-scatter.2.cloned.1.call-done = bf16[1024,512]{1,0:T(8,128)(2,1)} async-done(((bf16[1024,2048]{1,0:T(8,128)(2,1)}), bf16[1024,512]{1,0:T(8,128)(2,1)}) %reduce-scatter.2.cloned.1.call-update) | async-done | bytes 1048592 | tf_op jit(solution)/shard_map/reduce_scatter | solution.py:152
  637.2 2.5 add_convert_fusion
  (170 shorter events, 61.1 us)
Async XLA Ops:
  6.5 75.3 %copy-start = (bf16[4,64,64]{2,1,0:T(8,128)(2,1)S(1)}, bf16[4,64,64]{2,1,0:T(8,128)(2,1)}, u32[]{:S(2)}) copy-start(bf16[4,64,64]{2,1,0:T(8,128)(2,1)} %param.28) | copy-start | bytes 98308
  6.5 69.2 %copy-start.17 = (f32[2048]{0:T(1024)S(1)}, f32[2048]{0:T(1024)}, u32[]{:S(2)}) copy-start(f32[2048]{0:T(1024)} %param.22) | copy-start | bytes 24580
  6.5 39.6 %all-gather.16.cloned.1.call-start = ((), (), s32[]{:S(2)}) async-start(), calls=%async_computation.2 | async-start | bytes 5242880 | tf_op jit(solution)/shard_map/all_gather | solution.py:73
  7.3 68.4 %all-gather.18.cloned.1.call-start = ((), (), s32[]{:S(2)}) async-start(), calls=%async_computation.3 | async-start | bytes 1310720 | tf_op jit(solution)/shard_map/all_gather | solution.py:76
  9.1 175.7 %all-gather.20.cloned.1.call-start = ((), (), s32[]{:S(2)}) async-start(), calls=%async_computation.4 | async-start | bytes 1310720 | tf_op jit(solution)/shard_map/all_gather | solution.py:79
  11.0 178.8 %all-gather.24.cloned.1.call-start = ((), (), s32[]{:S(2)}) async-start(), calls=%async_computation.6 | async-start | bytes 1310720 | tf_op jit(solution)/shard_map/all_gather | solution.py:106
  12.9 207.8 %all-gather.22.cloned.1.call-start = ((), (), s32[]{:S(2)}) async-start(), calls=%async_computation.5 | async-start | bytes 2621440 | tf_op jit(solution)/shard_map/all_gather | solution.py:105
  49.2 30.3 %copy-start.9 = (f32[1024]{0:T(1024)}, f32[1024]{0:T(1024)S(1)}, u32[]{:S(2)}) copy-start(f32[1024]{0:T(1024)S(1)} %add_rsqrt_fusion.1) | copy-start | bytes 12292
  80.0 4.7 copy-start.16
  81.1 0.8 copy-start.6
  182.2 2.7 copy-start.10
  182.2 2.7 copy-start.15
  182.2 2.7 copy-start.18
  184.9 8.5 %copy-start.11 = (f32[1,512]{1,0:T(1,128)S(1)}, f32[1,512]{1,0:T(1,128)}, u32[]{:S(2)}) copy-start(f32[1,512]{1,0:T(1,128)} %param.32) | copy-start | bytes 6148
  189.7 27.1 %all-to-all-start = ((bf16[256,4,512]{0,2,1:T(8,128)(2,1)}), bf16[256,4,512]{0,2,1:T(8,128)(2,1)S(1)}, u32[]{:S(2)}, u32[]{:S(2)}) async-start(bf16[256,4,512]{0,2,1:T(8,128)(2,1)} %bitcast.106), calls=%async_computation | async-start | bytes 2097152 | tf_op jit(solution)/shard_map/all_to_all | solution.py:107
  193.3 78.8 %all-gather.26.cloned.1.call-start = ((), (), s32[]{:S(2)}) async-start(), calls=%async_computation.7 | async-start | bytes 5242880 | tf_op jit(solution)/shard_map/all_gather | solution.py:128
  216.9 3.8 copy-start.5
  222.2 6.8 %copy-start.3 = (f32[512,1408]{1,0:T(8,128)S(1)}, f32[512,1408]{1,0:T(8,128)}, u32[]{:S(2)}) copy-start(f32[512,1408]{1,0:T(8,128)} %param.34) | copy-start | bytes 8650756
  229.0 141.3 %all-gather.28.cloned.1.call-start = ((), (), s32[]{:S(2)}) async-start(), calls=%async_computation.8 | async-start | bytes 7208960 | tf_op jit(solution)/shard_map/all_gather | solution.py:133
  230.3 3.5 copy-start.4
  230.3 4.9 copy-start.13
  230.4 17.1 %copy-start.14 = (f32[1,352]{1,0:T(1,128)S(1)}, f32[1,352]{1,0:T(1,128)}, u32[]{:S(2)}) copy-start(f32[1,352]{1,0:T(1,128)} %param.37) | copy-start | bytes 4228
  230.4 29.3 %copy-start.12 = (f32[1,512]{1,0:T(1,128)S(1)}, f32[1,512]{1,0:T(1,128)}, u32[]{:S(2)}) copy-start(f32[1,512]{1,0:T(1,128)} %param.41) | copy-start | bytes 6148
  230.4 41.6 %copy-start.7 = (f32[3,1408]{1,0:T(4,128)S(1)}, f32[3,1408]{1,0:T(4,128)}, u32[]{:S(2)}) copy-start(f32[3,1408]{1,0:T(4,128)} %param.39) | copy-start | bytes 50692
  230.4 41.6 %copy-start.8 = (f32[3,1408]{1,0:T(4,128)S(1)}, f32[3,1408]{1,0:T(4,128)}, u32[]{:S(2)}) copy-start(f32[3,1408]{1,0:T(4,128)} %param.38) | copy-start | bytes 50692
  230.4 246.4 %all-gather.30.cloned.1.call-start = ((), (), s32[]{:S(2)}) async-start(), calls=%async_computation.9 | async-start | bytes 7208960 | tf_op jit(solution)/shard_map/all_gather | solution.py:134
  233.8 136.5 %copy-start.19 = (f32[2048]{0:T(1024)S(1)}, f32[2048]{0:T(1024)}, u32[]{:S(2)}) copy-start(f32[2048]{0:T(1024)} %param.33) | copy-start | bytes 24580
  233.8 349.6 %all-gather.32.cloned.1.call-start = ((), (), s32[]{:S(2)}) async-start(), calls=%async_computation.10 | async-start | bytes 7208960 | tf_op jit(solution)/shard_map/all_gather | solution.py:147
  235.1 402.0 %reduce-scatter.2.cloned.1.call-start = ((), (), s32[]{:S(2)}) async-start(), calls=%async_computation.11 | async-start | bytes 5242880 | tf_op jit(solution)/shard_map/reduce_scatter | solution.py:152
  511.3 125.9 %copy-start.2 = (bf16[1024,512]{1,0:T(8,128)(2,1)S(1)}, bf16[1024,512]{1,0:T(8,128)(2,1)}, u32[]{:S(2)}) copy-start(bf16[1024,512]{1,0:T(8,128)(2,1)} %add_convert_fusion.1) | copy-start | bytes 3145732
  583.4 56.3 %copy-start.1 = (bf16[4,64,64]{2,1,0:T(8,128)(2,1)S(1)}, bf16[4,64,64]{2,1,0:T(8,128)(2,1)}, u32[]{:S(2)}) copy-start(bf16[4,64,64]{2,1,0:T(8,128)(2,1)} %param.28) | copy-start | bytes 98308
Sparse Core Ops, SparseCore 0:
  8.9 37.1 all-gather.15
  47.7 27.9 all-gather.17
  77.3 27.3 all-gather.19
  106.1 27.3 all-gather.23
  189.8 30.8 all-gather.21
  229.1 32.8 all-gather.25
  263.6 106.6 all-gather.27
  371.9 104.9 all-gather.29
  478.4 104.9 all-gather.31
  594.5 42.6 reduce-scatter.1
where the time goes:
time: 649 us; the launch traced here: 647 us
  waiting for transfers between devices  356 us (55%)
  local copies, waits for them, and re-layouts  76.1 us (12%)
  other arithmetic  73.7 us (11%)
  blocking collectives  68.5 us (11%)
  matrix products  53.7 us (8%)
  between operations  14.1 us (2%)
    all_gather x1, waiting for transfers between devices, per_device(): lax.all_gather(upgate_bf, 'fs', axis=0, tiled=True)  94.8 us
    all_gather x1, waiting for transfers between devices, per_device(): lax.all_gather(upval_bf, 'fs', axis=0, tiled=True)  94.6 us
    all_gather x1, waiting for transfers between devices, per_device(): lax.all_gather(down_weight.astype(jnp.bfloat16), 'fs', axis=1, tiled=True)  72.1 us
    slice x53, local copies, waits for them, and re-layouts, run_scan(): _, states = lax.associative_scan(combine_pairs, pair, axis=1)  56.2 us
    reduce_scatter x1, waiting for transfers between devices, per_device(): lax.psum_scatter(ffn_terms, 'tp', scatter_dimension=1, tiled=True)  42.8 us
    all_gather x1, waiting for transfers between devices, per_device(): lax.all_gather(branch_weight.astype(jnp.bfloat16), 'fs', axis=0, tiled=True)  26.5 us
    add x1, other arithmetic, causal_mix(): totals = totals + padded[:, k:k + seq_len] * filter_taps[k]  16 us
  transfers between devices with their start and end apart: 11, of which 8 were waited for; matrix products, arithmetic and copies ran while one was open for 28% of the time, Pallas kernels for 0%

commit v1 on v0

v1 whole, which is shorter than its diff:
```python
import functools

import jax
import jax.numpy as jnp
from jax import lax
from jax.experimental import pallas as pl
from jax.experimental.pallas import tpu as pltpu
from jax.sharding import PartitionSpec as P

SEQ_LEN = 512
MESH = pl.DeviceIdType.MESH
VMEM = pl.BlockSpec(memory_space=pltpu.VMEM)
CHUNKS = 4


def expand_scale(gathered):
    return gathered.T.reshape(-1)


def causal_mix(values, filter_taps, seq_len):
    columns = values.shape[-1]
    grouped = values.reshape(-1, seq_len, columns)
    tap_count = filter_taps.shape[0]
    padded = jnp.pad(grouped, ((0, 0), (tap_count - 1, 0), (0, 0)))
    totals = padded[:, 0:seq_len] * filter_taps[0]
    for k in range(1, tap_count):
        totals = totals + padded[:, k : k + seq_len] * filter_taps[k]
    return totals.reshape(-1, columns)


def mixer_kernel(branch_ref, gelu_ref, bscale_ref, gscale_ref, taps_ref, rg_ref, ig_ref, sp_ref, out_ref):
    branch = branch_ref[...] * bscale_ref[...]
    rows = branch.shape[0]
    position = lax.broadcasted_iota(jnp.int32, branch.shape, 0)

    def delayed(values, shift, fill):
        return jnp.where(position >= shift, pltpu.roll(values, shift, 0), fill)

    taps = taps_ref.shape[0]
    conv = branch * taps_ref[taps - 1 : taps, :]
    for k in range(taps - 1):
        conv = conv + delayed(branch, taps - 1 - k, 0.0) * taps_ref[k : k + 1, :]
    conv_bf = conv.astype(jnp.bfloat16)
    conv = conv_bf.astype(jnp.float32)
    recur = jax.nn.sigmoid(jnp.dot(conv_bf, rg_ref[...], preferred_element_type=jnp.float32))
    rate = jax.nn.sigmoid(jnp.dot(conv_bf, ig_ref[...], preferred_element_type=jnp.float32))
    log_decay = -8.0 * recur * sp_ref[...]
    factor = jnp.exp(log_decay)
    state = jnp.sqrt(-jnp.tanh(log_decay) * (factor * factor + 1.0)) * rate * conv
    shift = 1
    while shift < rows:
        state = factor * delayed(state, shift, 0.0) + state
        factor = factor * delayed(factor, shift, 1.0)
        shift *= 2
    gelu_in = gelu_ref[...] * gscale_ref[...]
    out_ref[...] = (state * jax.nn.gelu(gelu_in)).astype(jnp.bfloat16)


def block_diagonal(gate, per):
    count, width, _ = gate.shape
    grouped = gate.reshape(count // per, per, width, width)
    eye = jnp.eye(per, dtype=gate.dtype)
    return jnp.einsum("gpab,pq->gpaqb", grouped, eye).reshape(count // per, per * width, per * width)


def mixer(branch, gelu_in, bscale, gscale, taps, recur_gate, input_gate, softplus):
    rows, channels = branch.shape
    lanes = min(channels, 128)
    per = lanes // recur_gate.shape[1]
    rg, ig = block_diagonal(recur_gate, per), block_diagonal(input_gate, per)
    tile = pl.BlockSpec((SEQ_LEN, lanes), lambda s, c: (s, c))
    row = pl.BlockSpec((1, lanes), lambda s, c: (0, c))
    gate = pl.BlockSpec((None, lanes, lanes), lambda s, c: (c, 0, 0))
    return pl.pallas_call(
        mixer_kernel,
        grid=(rows // SEQ_LEN, channels // lanes),
        out_shape=jax.ShapeDtypeStruct((rows, channels), jnp.bfloat16),
        in_specs=[
            tile, tile, row, row,
            pl.BlockSpec((taps.shape[0], lanes), lambda s, c: (0, c)),
            gate, gate, row,
        ],
        out_specs=tile,
        cost_estimate=pl.CostEstimate(flops=10**8, bytes_accessed=10 * rows * channels, transcendentals=rows * channels * 6),
    )(branch, gelu_in, bscale[None], gscale[None], taps, rg, ig, softplus[None])


class Across:
    def __init__(self, tp, src, held, local_sem, pair_sems, sends, recvs, fsends, frecvs):
        self.src, self.held, self.local_sem, self.pair_sems = src, held, local_sem, pair_sems
        self.sems = (sends, recvs, fsends, frecvs)
        self.me = lax.axis_index("tp")
        self.core, self.chips = lax.rem(self.me, 2), tp // 2
        self.chip = self.me // 2
        self.partner = self.me + 1 - 2 * self.core
        self.rows = src.shape[0] // CHUNKS
        self.others = [
            lax.rem(self.chip + d, self.chips) * 2 + self.core for d in range(1, self.chips)]
        self.open = []

    def copy(self, source, dest, send, recv, device):
        return pltpu.make_async_remote_copy(
            src_ref=source, dst_ref=dest, send_sem=send, recv_sem=recv,
            device_id={"tp": device}, device_id_type=MESH)

    def start_part(self, k):
        part = pl.ds(k * self.rows, self.rows)
        for d in range(1, self.chips):
            copy = self.copy(
                self.src.at[part], self.held.at[self.me, part], self.sems[0].at[d - 1, k],
                self.sems[1].at[d - 1, k], self.others[d - 1])
            copy.start()
            self.open.append(copy.wait_send)

    def start_own(self):
        own = pltpu.make_async_copy(self.src, self.held.at[self.me], self.local_sem)
        own.start()
        pair = self.copy(
            self.src, self.held.at[self.me], self.pair_sems.at[0], self.pair_sems.at[1],
            self.partner)
        pair.start()
        self.open += [own.wait, pair.wait]

    def forward(self, k):
        part = pl.ds(k * self.rows, self.rows)
        for d in range(1, self.chips):
            source = lax.rem(self.chip - d + self.chips, self.chips) * 2 + self.core
            self.copy(
                self.src.at[part], self.held.at[source, part], self.sems[0].at[d - 1, k],
                self.sems[1].at[d - 1, k], self.others[d - 1]).wait_recv()
            onward = self.copy(
                self.held.at[source, part], self.held.at[source, part],
                self.sems[2].at[d - 1, k], self.sems[3].at[d - 1, k], self.partner)
            onward.start()
            self.open.append(onward.wait)

    def finish(self):
        for wait in self.open:
            wait()


def across_scratch(tp, rows, columns):
    many = pltpu.SemaphoreType.DMA((tp // 2 - 1, CHUNKS))
    return [
        pltpu.VMEM((tp, rows, columns), jnp.bfloat16),
        pltpu.SemaphoreType.DMA, pltpu.SemaphoreType.DMA((2,)), many, many, many, many,
    ]


class Along:
    def __init__(self, fs, src, out, sems, local_sem):
        self.fs, self.src, self.out, self.sems, self.local_sem = fs, src, out, sems, local_sem
        self.z, self.y = lax.axis_index("fs"), lax.axis_index("grp")

    def cases(self, s):
        z, fs = self.z, self.fs
        return (
            (0, (z >= s - 1) & (z <= fs - 2), z - s + 1, z + 1, z >= s, z - s),
            (1, (z >= 1) & (z <= fs - s), z + s - 1, z - 1, z <= fs - 1 - s, z + s),
        )

    def hop(self, s, way, shard, device):
        source = self.src.at[self.y] if s == 1 else self.out.at[shard, self.y]
        return pltpu.make_async_remote_copy(
            src_ref=source, dst_ref=self.out.at[shard, self.y],
            send_sem=self.sems.at[0, way, s - 1], recv_sem=self.sems.at[1, way, s - 1],
            device_id={"fs": device}, device_id_type=MESH)

    def swap(self, s, way, shard, half):
        where = self.out.at[shard, half]
        return pltpu.make_async_remote_copy(
            src_ref=where, dst_ref=where,
            send_sem=self.sems.at[2, way, s - 1], recv_sem=self.sems.at[3, way, s - 1],
            device_id={"grp": 1 - self.y}, device_id_type=MESH)

    def start(self):
        self.own = pltpu.make_async_copy(self.src, self.out.at[self.z], self.local_sem)
        self.send(1)
        self.own.start()

    def send(self, s):
        for way, sends, shard, device, _, _ in self.cases(s):
            @pl.when(sends)
            def _():
                self.hop(s, way, shard, device).start()

    def pump(self, s):
        for way, _, _, _, gets, shard in self.cases(s):
            @pl.when(gets)
            def _():
                self.hop(s, way, shard, self.z + 1 - 2 * way).wait_recv()
                if s + 1 < self.fs:
                    nways = self.cases(s + 1)[way]

                    @pl.when(nways[1])
                    def _():
                        self.hop(s + 1, way, nways[2], nways[3]).start()
                self.swap(s, way, shard, self.y).start()

    def finish(self):
        self.own.wait()
        for s in range(1, self.fs):
            for way, sends, sent, device, gets, shard in self.cases(s):
                @pl.when(sends)
                def _():
                    self.hop(s, way, sent, device).wait_send()

                @pl.when(gets)
                def _():
                    self.swap(s, way, shard, self.y).wait_send()
                    self.swap(s, way, shard, 1 - self.y).wait_recv()


def along_scratch(fs):
    return [pltpu.SemaphoreType.DMA((4, 2, fs - 1)), pltpu.SemaphoreType.DMA]


def greet(tp, fs):
    me, z, y = lax.axis_index("tp"), lax.axis_index("fs"), lax.axis_index("grp")
    core, chip, chips = lax.rem(me, 2), me // 2, tp // 2
    barrier = pltpu.get_barrier_semaphore()
    devices = [{"tp": me + 1 - 2 * core}, {"grp": 1 - y}]
    devices += [{"tp": lax.rem(chip + d, chips) * 2 + core} for d in range(1, chips)]
    devices += [{"fs": lax.rem(z + d, fs)} for d in range(1, fs)]
    for device in devices:
        pl.semaphore_signal(barrier, inc=1, device_id=device, device_id_type=MESH)
    pl.semaphore_wait(barrier, len(devices))


def norm_rows(tp, held, gain, out):
    _, rows, columns = held.shape
    step = 128

    def body(i, carry):
        part = pl.ds(pl.multiple_of(i * step, step), step)
        total = jnp.zeros((step, 1), jnp.float32)
        for q in range(tp):
            values = held[q, part, :].astype(jnp.float32)
            total = total + jnp.sum(values * values, axis=-1, keepdims=True)
        inverse = lax.rsqrt(total / (tp * columns) + 1e-06)
        for q in range(tp):
            cols = slice(q * columns, (q + 1) * columns)
            values = held[q, part, :].astype(jnp.float32)
            out[part, cols] = (values * inverse * gain[:, cols]).astype(jnp.bfloat16)
        return carry

    lax.fori_loop(0, rows // step, body, 0)


def first_kernel(tp, fs, tokens, gain, mixer_src, scale_src, normed, mixers, scales, *scratch):
    across = Across(tp, tokens, *scratch[:7])
    along = Along(fs, mixer_src, mixers, *scratch[7:9])
    scale_sems, scale_local = scratch[9:]
    greet(tp, fs)
    z = lax.axis_index("fs")
    along.start()
    for k in range(CHUNKS):
        across.start_part(k)
    across.start_own()
    own = pltpu.make_async_copy(scale_src, scales.at[z], scale_local)
    own.start()
    small = []
    for d in range(1, fs):
        small.append(pltpu.make_async_remote_copy(
            src_ref=scale_src, dst_ref=scales.at[z], send_sem=scale_sems.at[0, d - 1],
            recv_sem=scale_sems.at[1, d - 1], device_id={"fs": lax.rem(z + d, fs)},
            device_id_type=MESH))
        small[-1].start()
    for k in range(CHUNKS):
        across.forward(k)
        if k + 1 < fs:
            along.pump(k + 1)
    for s in range(CHUNKS + 1, fs):
        along.pump(s)
    across.finish()
    norm_rows(tp, across.held, gain, normed)
    own.wait()
    for copy in small:
        copy.wait()
    along.finish()


ANY = pl.BlockSpec(memory_space=pl.ANY)


def first(tp, fs, tokens, gain, mixer_src, scale_src):
    rows, columns = tokens.shape
    return pl.pallas_call(
        functools.partial(first_kernel, tp, fs),
        out_shape=(
            jax.ShapeDtypeStruct((rows, columns * tp), jnp.bfloat16),
            jax.ShapeDtypeStruct((fs,) + mixer_src.shape, jnp.bfloat16),
            jax.ShapeDtypeStruct((fs,) + scale_src.shape, jnp.float32),
        ),
        in_specs=[VMEM] * 4, out_specs=(VMEM, ANY, VMEM),
        scratch_shapes=across_scratch(tp, rows, columns) + along_scratch(fs) + [
            pltpu.SemaphoreType.DMA((2, fs - 1)), pltpu.SemaphoreType.DMA],
        compiler_params=pltpu.CompilerParams(
            collective_id=0, has_side_effects=True, vmem_limit_bytes=40 * 2**20),
        cost_estimate=pl.CostEstimate(flops=10**7, bytes_accessed=60 * 2**20, transcendentals=0),
        name="first",
    )(tokens, gain[None], mixer_src, scale_src)


def second_kernel(
    tp, fs, state, weight, scale, tokens, gain, val_src, down_src, hidden, normed, val_out,
    down_out, *scratch,
):
    states = Across(tp, state, *scratch[:7])
    hiddens = Across(tp, hidden, *scratch[7:14])
    val = Along(fs, val_src, val_out, *scratch[14:16])
    down = Along(fs, down_src, down_out, *scratch[16:18])
    greet(tp, fs)
    val.start()
    for k in range(CHUNKS):
        states.start_part(k)
    states.start_own()
    down.start()
    for k in range(CHUNKS):
        states.forward(k)
    states.finish()
    held, columns = states.held, state.shape[1]
    step = tokens.shape[0] // CHUNKS
    for k in range(CHUNKS):
        part = pl.ds(k * step, step)
        mixed = jnp.zeros((step, tokens.shape[1]), jnp.float32)
        for q in range(tp):
            term = jnp.dot(
                held[q, part, :], weight[q * columns : (q + 1) * columns, :],
                preferred_element_type=jnp.float32) * scale[...]
            mixed = mixed + term.astype(jnp.bfloat16).astype(jnp.float32)
        hidden[part, :] = (tokens[part, :].astype(jnp.float32) + mixed).astype(jnp.bfloat16)
        hiddens.start_part(k)
    hiddens.start_own()
    val.pump(1)
    hiddens.forward(0)
    hiddens.forward(1)
    down.pump(1)
    for k in range(2, CHUNKS):
        hiddens.forward(k)
    if fs > 2:
        val.pump(2)
    hiddens.finish()
    norm_rows(tp, hiddens.held, gain, normed)
    if fs > 2:
        down.pump(2)
    for s in range(3, fs):
        val.pump(s)
        down.pump(s)
    val.finish()
    down.finish()


def second(tp, fs, state, weight, scale, tokens, gain, val_src, down_src):
    rows, columns = tokens.shape
    return pl.pallas_call(
        functools.partial(second_kernel, tp, fs),
        out_shape=(
            jax.ShapeDtypeStruct((rows, columns), jnp.bfloat16),
            jax.ShapeDtypeStruct((rows, columns * tp), jnp.bfloat16),
            jax.ShapeDtypeStruct((fs,) + val_src.shape, jnp.bfloat16),
            jax.ShapeDtypeStruct((fs,) + down_src.shape, jnp.bfloat16),
        ),
        in_specs=[VMEM] * 7, out_specs=(VMEM, VMEM, ANY, ANY),
        scratch_shapes=across_scratch(tp, rows, state.shape[1]) + across_scratch(tp, rows, columns)
        + along_scratch(fs) + along_scratch(fs),
        compiler_params=pltpu.CompilerParams(
            collective_id=1, has_side_effects=True, vmem_limit_bytes=48 * 2**20),
        cost_estimate=pl.CostEstimate(flops=10**9, bytes_accessed=180 * 2**20, transcendentals=0),
        name="second",
    )(state, weight, scale[None], tokens, gain[None], val_src, down_src)


def half_rows(weight):
    count = lax.axis_size("grp")
    rows = weight.shape[0] // count
    start = lax.axis_index("grp") * rows
    return lax.dynamic_slice_in_dim(weight, start, rows, 0).astype(jnp.bfloat16)


def whole_rows(weight):
    return lax.all_gather(half_rows(weight), ("fs", "grp"), axis=0, tiled=True)


def halves(weight):
    count = lax.axis_size("grp")
    return weight.astype(jnp.bfloat16).reshape(count, weight.shape[0] // count, weight.shape[1])


def per_device(
    tokens, mixer_gain, branch_weight, gelu_weight, branch_scale, gelu_scale, branch_taps,
    recur_gate, input_gate, decay_param, out_weight, out_scale, ffn_gain, upgate_weight,
    upval_weight, upgate_scale, upval_scale, upgate_taps, upval_taps, down_weight, down_scale,
):
    tp = lax.axis_size("tp")
    fs = lax.axis_size("fs")
    gate_full = whole_rows(upgate_weight)
    scale_list = (branch_scale, gelu_scale, out_scale, upgate_scale, upval_scale, down_scale)
    lru = branch_weight.shape[1]
    depth = branch_weight.shape[0] // 2
    mixer_src = jnp.concatenate(
        [halves(branch_weight), halves(gelu_weight), halves(out_weight.reshape(-1, lru))], axis=1)
    normed, mixers, packed = first(
        tp, fs, tokens, mixer_gain, mixer_src, jnp.concatenate(scale_list, axis=1))
    packed = packed[:, 0]
    scales, start = [], 0
    for piece in scale_list:
        scales.append(expand_scale(packed[:, start : start + piece.shape[1]]))
        start += piece.shape[1]
    rows_branch = mixers[:, :, :depth].reshape(-1, lru)
    rows_gelu = mixers[:, :, depth : 2 * depth].reshape(-1, lru)
    out_blocks = mixers[:, :, 2 * depth :].reshape((fs,) + out_weight.shape)
    branch = jnp.dot(normed, rows_branch, preferred_element_type=jnp.float32)
    gelu_in = jnp.dot(normed, rows_gelu, preferred_element_type=jnp.float32)
    gated_state = mixer(
        branch, gelu_in, scales[0], scales[1], branch_taps, recur_gate, input_gate,
        jax.nn.softplus(-decay_param))
    row_block = jnp.transpose(out_blocks, (1, 0, 2)).reshape(out_weight.shape[0], -1)
    own_columns = lax.all_to_all(row_block, "tp", split_axis=1, concat_axis=0, tiled=True)
    width = tokens.shape[1]
    own_scales = lax.dynamic_slice_in_dim(scales[2], lax.axis_index("tp") * width, width, 0)
    hidden_state, normed_ffn, value_full, down_blocks = second(
        tp, fs, gated_state, own_columns, own_scales, tokens, ffn_gain,
        halves(upval_weight), halves(down_weight))
    value_full = value_full.reshape(-1, upval_weight.shape[1])
    down_blocks = down_blocks.reshape((fs,) + down_weight.shape)
    up_gate = jnp.dot(normed_ffn, gate_full, preferred_element_type=jnp.float32)
    up_val = jnp.dot(normed_ffn, value_full, preferred_element_type=jnp.float32)
    conv_gate = causal_mix(up_gate * scales[3], upgate_taps, SEQ_LEN)
    conv_val = causal_mix(up_val * scales[4], upval_taps, SEQ_LEN)
    ffn_hidden = (jax.nn.silu(conv_gate) * conv_val).astype(jnp.bfloat16)
    piece = down_blocks.shape[2]
    terms = []
    for f in range(down_blocks.shape[0]):
        term = jnp.dot(ffn_hidden, down_blocks[f], preferred_element_type=jnp.float32)
        terms.append((term * scales[5][f * piece : (f + 1) * piece]).astype(jnp.bfloat16))
    ffn_terms = jnp.concatenate(terms, axis=1)
    ffn_sum = lax.psum_scatter(ffn_terms, "tp", scatter_dimension=1, tiled=True).astype(jnp.float32)
    return (hidden_state.astype(jnp.float32) + ffn_sum).astype(jnp.bfloat16)


def solution(mesh):
    in_specs = (
        P(("grp", "fs"), "tp"), P(), P("fs", "tp"), P("fs", "tp"), P("fs", "tp"), P("fs", "tp"),
        P(None, "tp"), P("tp", None, None), P("tp", None, None), P("tp"), P("tp", "fs"),
        P("fs", None), P(), P("fs", "tp"), P("fs", "tp"), P("fs", "tp"), P("fs", "tp"),
        P(None, "tp"), P(None, "tp"), P("tp", "fs"), P("fs", None),
    )
    return jax.shard_map(
        per_device, mesh=mesh, in_specs=in_specs, out_specs=P(("grp", "fs"), "tp"), check_vma=False
    )
```

time: 649 us -> 356 us (0.55)
  waiting for transfers between devices: 356 us -> 42 us
  Pallas kernels: 0 us -> 203 us
  blocking collectives: 68.5 us -> 0 us
  other arithmetic: 73.7 us -> 15.8 us
  local copies, waits for them, and re-layouts: 76.1 us -> 39.1 us
  matrix products: 53.7 us -> 37.3 us
    all_gather x9 -> x1, waiting for transfers between devices: 302 us -> 0.02 us  [whole_rows(): return lax.all_gather(half_rows(weight), ('fs', 'grp'), axis=0, tiled=True)]
    pallas_call x0 -> x3, Pallas kernels: none -> 203 us  [the longest x1 120 us: second(): pl.pallas_call(functools.partial(second_kernel, tp, fs), out_shape=(jax.S...]
    all_gather x6 -> x0, blocking collectives: 68.5 us -> none  [the longest x1 12.8 us: per_device(): lax.all_gather(branch_scale, 'fs', axis=0, tiled=True)]
    slice x53 -> x7, local copies, waits for them, and re-layouts: 56.2 us -> 13 us  [the longest x5 6.21 us: per_device(): scales[5][f * piece:(f + 1) * piece]]
    add x19 -> x0, other arithmetic: 28 us -> none  [the longest x1 16 us: causal_mix(): totals = totals + padded[:, k:k + seq_len] * filter_taps[k]]
    dot_general x9 -> x6, matrix products: 29.8 us -> 18.3 us  [the longest x4 8.6 us: per_device(): jnp.dot(ffn_hidden, down_blocks[f], preferred_element_type=jnp.float32)]
    mul x8 -> x0, other arithmetic: 11.3 us -> none  [the longest x7 10.6 us: combine_pairs(): return (earlier[0] * later[0], later[0] * earlier[1] + later[1])]
    all_to_all x1, waiting for transfers between devices: 11 us -> 0.01 us  [per_device(): lax.all_to_all(row_block, 'tp', split_axis=1, concat_axis=0, tiled=True)]
  transfers between devices with their start and end apart: 11 -> 3, of which waited for: 8 -> 1; matrix products, arithmetic and copies ran while one was open for 28% -> 15% of each run, Pallas kernels for 0% -> 57%
where the time goes in v1:
time: 356 us; the launch traced here: 355 us
  Pallas kernels  203 us (57%)
  waiting for transfers between devices  42 us (12%)
  local copies, waits for them, and re-layouts  39.1 us (11%)
  matrix products  37.3 us (10%)
  other arithmetic  15.8 us (4%)
  between operations  13.9 us (4%)
  starting transfers between devices  3.59 us (1%)
    pallas_call x1, Pallas kernels, second(): pl.pallas_call(functools.partial(second_kernel, tp, fs), out_shape=(jax.S...  120 us
    pallas_call x1, Pallas kernels, first(): pl.pallas_call(functools.partial(first_kernel, tp, fs), out_shape=(jax.Sh...  77.9 us
    reduce_scatter x1, waiting for transfers between devices, per_device(): lax.psum_scatter(ffn_terms, 'tp', scatter_dimension=1, tiled=True)  42 us
    dot_general x1, matrix products, per_device(): up_gate = jnp.dot(normed_ffn, gate_full, preferred_element_type=jnp.float32)  10.6 us
    dot_general x4, matrix products, per_device(): jnp.dot(ffn_hidden, down_blocks[f], preferred_element_type=jnp.float32)  8.6 us
    dot_general x1, matrix products, per_device(): up_val = jnp.dot(normed_ffn, value_full, preferred_element_type=jnp.float32)  8.43 us
  transfers between devices with their start and end apart: 3, of which 1 were waited for; matrix products, arithmetic and copies ran while one was open for 15% of the time, Pallas kernels for 57%

profile of v1, /device:TPU:0, one launch (start us, length us, event | category | flops | bytes accessed | tf_op | source)
XLA Modules:
  0.0 354.7 jit_solution(10992001108654541357)
XLA Ops:
  6.6 0.0 all-gather.2.cloned.1.call-start
  6.6 1.7 copy-done
  8.4 0.9 dynamic-slice_convert_fusion
  9.3 1.2 convert_element_type.59
  10.5 0.1 convert_element_type.60
  10.6 1.1 convert_element_type.57
  11.7 0.1 concatenate.10.scale_src
  11.9 0.1 pad_maximum_fusion.1.mixer_src
  11.9 77.9 %first.1 = (bf16[1024,2048]{1,0:T(8,128)(2,1)S(1)}, bf16[4,2,768,256]{3,2,1,0:T(8,128)(2,1)S(1)}, f32[4,1,1856]{2,1,0:T(1,128)S(1)}) custom-call(bf16[1024,512]{1,0:T(8,128)(2,1)S(1)} %copy-done.2, f32[1,2048]{1,0:T(1,128)S(1)} %bitcast.68, bf16[2,768,256]{2,1,0:T(8,128)(2,1)S(1)} %pad_maximum_fusion.1.mixer_src, f32[1,1856]{1,0:T(1,128)S(1)} %concatenate.10.scale_src), custom_call_target="tpu_custom_call" | custom-call | flops 10000000 | bytes 62914560 | tf_op jit(solution)/shard_map/first/pallas_call | solution.py:288
  89.9 1.7 fusion.1
  91.6 0.9 copy-done.7
  92.5 1.2 reshape.104
  93.7 3.5 all-to-all-start
  97.2 0.0 reduce-scatter.2.cloned.1.call-start
  97.3 0.1 slice_bitcast_fusion.4
  97.4 0.1 copy.28
  97.5 0.7 broadcast_in_dim_reshape.8.bscale_ref
  98.2 0.1 copy.29
  98.3 0.6 broadcast_in_dim_reshape.9.gscale_ref
  98.9 0.3 multiply_bitcast_fusion
  99.2 0.7 reshape.100.rg_ref
  100.0 0.7 reshape.103.ig_ref
  100.7 0.1 slice_bitcast_fusion
  100.8 0.1 copy.30
  100.9 0.8 reshape.105
  101.7 0.6 fusion.2
  102.3 0.1 slice_bitcast_fusion.3
  102.4 5.0 %fusion.4.gelu_ref = f32[1024,256]{1,0:T(8,128)} fusion(bf16[1024,2048]{1,0:T(8,128)(2,1)} %copy-done.7, bf16[2048,256]{1,0:T(8,128)(2,1)} %bitcast.84), kind=kOutput, calls=%fused_computation.32 | convolution fusion | flops 1073741824 | bytes 6291456 | tf_op jit(solution)/shard_map/dot_general | solution.py:414
  107.3 0.1 convert_element_type.61
  107.5 1.3 convert_element_type.62
  108.8 0.8 copy.32
  109.6 1.7 mul.156
  111.3 0.8 copy.31
  112.1 1.6 mul.143
  113.8 1.4 copy.33
  115.2 0.9 mul.169
  116.1 1.4 copy.35
  117.5 1.5 mul.172
  119.1 1.4 copy.37
  120.5 1.5 mul.175
  122.0 1.4 copy.39
  123.3 1.5 mul.178
  124.9 0.8 dynamic_slice.6
  125.6 1.2 compare_select_fusion
  126.8 4.7 %fusion.3.branch_ref = f32[1024,256]{1,0:T(8,128)} fusion(bf16[1024,2048]{1,0:T(8,128)(2,1)} %copy-done.7, bf16[2048,256]{1,0:T(8,128)(2,1)} %bitcast.83), kind=kOutput, calls=%fused_computation.31 | convolution fusion | flops 1073741824 | bytes 6291456 | tf_op jit(solution)/shard_map/dot_general | solution.py:413
  131.6 5.5 %shard_map.199.state = bf16[1024,256]{1,0:T(8,128)(2,1)} custom-call(f32[1024,256]{1,0:T(8,128)} %fusion.3.branch_ref, f32[1024,256]{1,0:T(8,128)} %fusion.4.gelu_ref, f32[1,256]{1,0:T(1,128)} %broadcast_in_dim_reshape.8.bscale_ref, f32[1,256]{1,0:T(1,128)} %broadcast_in_dim_reshape.9.gscale_ref, f32[4,256]{1,0:T(4,128)} %taps_ref.1, ...), custom_call_target="tpu_custom_call" | custom-call | flops 100000000 | bytes 2621440 | tf_op jit(solution)/shard_map/pallas_call | solution.py:74
  137.1 1.6 slice_reduce_fusion.2
  138.7 1.0 copy-done.4
  139.7 119.7 %second.1 = (bf16[1024,512]{1,0:T(8,128)(2,1)S(1)}, bf16[1024,2048]{1,0:T(8,128)(2,1)}, bf16[4,2,256,1408]{3,2,1,0:T(8,128)(2,1)}, bf16[4,2,704,512]{3,2,1,0:T(8,128)(2,1)}) custom-call(bf16[1024,256]{1,0:T(8,128)(2,1)S(1)} %copy-done.4, bf16[1024,512]{1,0:T(8,128)(2,1)S(1)} %bitcast.66, f32[1,512]{1,0:T(1,128)S(1)} %bitcast.67, ...), custom_call_target="tpu_custom_call" | custom-call | flops 1000000000 | bytes 188743680 | tf_op jit(solution)/shard_map/second/pallas_call | solution.py:356
  259.4 1.0 copy-done.3
  260.4 5.1 %fusion = (bf16[1,2,704,512]{3,2,1,0:T(8,128)(2,1)}, bf16[1,2,704,512]{3,2,1,0:T(8,128)(2,1)S(1)}, bf16[1,2,704,512]{3,2,1,0:T(8,128)(2,1)}, bf16[1,2,704,512]{3,2,1,0:T(8,128)(2,1)}) fusion(bf16[4,2,704,512]{3,2,1,0:T(8,128)(2,1)} %get-tuple-element.18), kind=kLoop, calls=%fused_computation.28 | loop fusion | bytes 11534336 | tf_op jit(solution)/shard_map/slice | solution.py:435
  265.5 0.5 copy-done.33
  266.0 1.6 copy-done.34
  267.5 8.4 %convolution_multiply_fusion = f32[1024,1408]{1,0:T(8,128)} fusion(bf16[1024,2048]{1,0:T(8,128)(2,1)S(1)} %copy-done.34, bf16[2048,1408]{1,0:T(8,128)(2,1)S(1)} %bitcast.91, f32[1408]{0:T(1024)S(1)} %copy-done.23), kind=kOutput, calls=%fused_computation.1 | convolution fusion | flops 5907021824 | bytes 15734272 | tf_op jit(solution)/shard_map/dot_general | solution.py:428
  276.0 0.0 all-gather.2.cloned.1.call-done
  276.1 10.6 %convolution_multiply_fusion.1 = f32[1024,1408]{1,0:T(8,128)S(1)} fusion(bf16[1024,2048]{1,0:T(8,128)(2,1)} %get-tuple-element.16, bf16[2048,1408]{1,0:T(8,128)(2,1)} %all-gather.2.cloned.1.call-done, f32[1408]{0:T(1024)S(1)} %copy-done.22), kind=kOutput, calls=%fused_computation.2 | convolution fusion | flops 5907021824 | bytes 15734272 | tf_op jit(solution)/shard_map/dot_general | solution.py:427
  286.7 5.3 %multiply_convert_fusion = bf16[2,512,1408]{2,1,0:T(8,128)(2,1)S(1)} fusion(f32[2,512,1408]{2,1,0:T(8,128)S(1)} %bitcast.70, f32[2,512,1408]{2,1,0:T(8,128)S(1)} %bitcast.71, f32[1408]{0:T(1024)S(1)} %copy-done.17, f32[1408]{0:T(1024)S(1)} %copy-done.18, f32[1408]{0:T(1024)S(1)} %copy-done.16, f32[1408]{0:T(1024)S(1)} %copy-done.20, f32[1408]{0:T(1024)S(1)} %copy-done.19, ...), kind=kLoop, calls=%fused_computation | loop fusion | flops 23068672 | bytes 14451712 | tf_op jit(solution)/shard_map/convert_element_type | solution.py:431
  292.1 3.3 multiply_convert_fusion.4
  295.4 1.8 multiply_convert_fusion.3
  297.2 1.8 multiply_convert_fusion.2
  299.0 1.8 multiply_convert_fusion.1
  300.8 2.4 pad_maximum_fusion
  303.1 42.0 %reduce-scatter.2.cloned.1.call-done = bf16[1024,512]{1,0:T(8,128)(2,1)} async-done(((bf16[1024,2048]{1,0:T(8,128)(2,1)}), bf16[1024,512]{1,0:T(8,128)(2,1)}) %reduce-scatter.2.cloned.1.call-update) | async-done | bytes 1048592 | tf_op jit(solution)/shard_map/reduce_scatter | solution.py:438
  345.1 2.8 add_convert_fusion
  (70 shorter events, 0.2 us)
Async XLA Ops:
  6.5 1.8 copy-start
  6.5 5.1 %copy-start.13 = (f32[512,256]{1,0:T(8,128)S(1)}, f32[512,256]{1,0:T(8,128)}, u32[]{:S(2)}) copy-start(f32[512,256]{1,0:T(8,128)} %param.24) | copy-start | bytes 1572868
  6.5 5.2 %copy-start.31 = (f32[1,64]{1,0:T(1,128)S(1)}, f32[1,64]{1,0:T(1,128)}, u32[]{:S(2)}) copy-start(f32[1,64]{1,0:T(1,128)} %param.25) | copy-start | bytes 772
  6.5 5.2 %copy-start.32 = (f32[1,64]{1,0:T(1,128)S(1)}, f32[1,64]{1,0:T(1,128)}, u32[]{:S(2)}) copy-start(f32[1,64]{1,0:T(1,128)} %param.26) | copy-start | bytes 772
  6.5 5.2 %copy-start.27 = (f32[1,512]{1,0:T(1,128)S(1)}, f32[1,512]{1,0:T(1,128)}, u32[]{:S(2)}) copy-start(f32[1,512]{1,0:T(1,128)} %param.32) | copy-start | bytes 6148
  6.5 5.2 %copy-start.29 = (f32[1,352]{1,0:T(1,128)S(1)}, f32[1,352]{1,0:T(1,128)}, u32[]{:S(2)}) copy-start(f32[1,352]{1,0:T(1,128)} %param.36) | copy-start | bytes 4228
  6.6 5.2 %copy-start.30 = (f32[1,352]{1,0:T(1,128)S(1)}, f32[1,352]{1,0:T(1,128)}, u32[]{:S(2)}) copy-start(f32[1,352]{1,0:T(1,128)} %param.37) | copy-start | bytes 4228
  6.6 5.2 %copy-start.28 = (f32[1,512]{1,0:T(1,128)S(1)}, f32[1,512]{1,0:T(1,128)}, u32[]{:S(2)}) copy-start(f32[1,512]{1,0:T(1,128)} %param.41) | copy-start | bytes 6148
  6.6 5.3 %copy-start.5 = (f32[2048]{0:T(1024)S(1)}, f32[2048]{0:T(1024)}, u32[]{:S(2)}) copy-start(f32[2048]{0:T(1024)} %param.22) | copy-start | bytes 24580
  6.6 269.4 %all-gather.2.cloned.1.call-start = ((), (), s32[]{:S(2)}) async-start(), calls=%async_computation.2 | async-start | bytes 6488064 | tf_op jit(solution)/shard_map/all_gather | solution.py:382
  9.3 2.6 copy-start.2
  89.9 2.7 copy-start.7
  89.9 9.0 %copy-start.14 = (bf16[4,64,64]{2,1,0:T(8,128)(2,1)S(1)}, bf16[4,64,64]{2,1,0:T(8,128)(2,1)}, u32[]{:S(2)}) copy-start(bf16[4,64,64]{2,1,0:T(8,128)(2,1)} %param.29) | copy-start | bytes 98308
  89.9 9.0 %copy-start.15 = (bf16[4,64,64]{2,1,0:T(8,128)(2,1)S(1)}, bf16[4,64,64]{2,1,0:T(8,128)(2,1)}, u32[]{:S(2)}) copy-start(bf16[4,64,64]{2,1,0:T(8,128)(2,1)} %param.28) | copy-start | bytes 98308
  93.7 45.0 %all-to-all-start = ((bf16[256,4,512]{2,0,1:T(8,128)(2,1)}), bf16[256,4,512]{2,0,1:T(8,128)(2,1)S(1)}, u32[]{:S(2)}, u32[]{:S(2)}) async-start(bf16[256,4,512]{2,0,1:T(8,128)(2,1)} %bitcast.14), calls=%async_computation | async-start | bytes 2097152 | tf_op jit(solution)/shard_map/all_to_all | solution.py:419
  97.2 247.9 %reduce-scatter.2.cloned.1.call-start = ((), (), s32[]{:S(2)}) async-start(), calls=%async_computation.3 | async-start | bytes 5242880 | tf_op jit(solution)/shard_map/reduce_scatter | solution.py:438
  101.7 5.7 %copy-start.9 = (f32[512,1408]{1,0:T(8,128)S(1)}, f32[512,1408]{1,0:T(8,128)}, u32[]{:S(2)}) copy-start(f32[512,1408]{1,0:T(8,128)} %param.35) | copy-start | bytes 8650756
  102.4 5.1 %copy-start.10 = (f32[1408,512]{1,0:T(8,128)S(1)}, f32[1408,512]{1,0:T(8,128)}, u32[]{:S(2)}) copy-start(f32[1408,512]{1,0:T(8,128)} %param.40) | copy-start | bytes 8650756
  126.8 11.8 %copy-start.6 = (f32[2048]{0:T(1024)S(1)}, f32[2048]{0:T(1024)}, u32[]{:S(2)}) copy-start(f32[2048]{0:T(1024)} %param.33) | copy-start | bytes 24580
  138.7 1.0 copy-start.4
  259.4 1.0 copy-start.3
  260.4 5.1 %copy-start.23 = (f32[1408]{0:T(1024)S(1)}, f32[1408]{0:T(1024)}, u32[]{:S(2)}) copy-start(f32[1408]{0:T(1024)} %mul.156) | copy-start | bytes 16900
  260.4 5.6 %copy-start.33 = (bf16[4,2,256,1408]{3,2,1,0:T(8,128)(2,1)S(1)}, bf16[4,2,256,1408]{3,2,1,0:T(8,128)(2,1)}, u32[]{:S(2)}) copy-start(bf16[4,2,256,1408]{3,2,1,0:T(8,128)(2,1)} %get-tuple-element.17) | copy-start | bytes 17301508
  260.4 7.2 %copy-start.34 = (bf16[1024,2048]{1,0:T(8,128)(2,1)S(1)}, bf16[1024,2048]{1,0:T(8,128)(2,1)}, u32[]{:S(2)}) copy-start(bf16[1024,2048]{1,0:T(8,128)(2,1)} %get-tuple-element.16) | copy-start | bytes 12582916
  267.5 8.5 %copy-start.22 = (f32[1408]{0:T(1024)S(1)}, f32[1408]{0:T(1024)}, u32[]{:S(2)}) copy-start(f32[1408]{0:T(1024)} %mul.143) | copy-start | bytes 16900
  276.0 10.7 %copy-start.16 = (f32[1408]{0:T(1024)S(1)}, f32[1408]{0:T(1024)}, u32[]{:S(2)}) copy-start(f32[1408]{0:T(1024)} %get-tuple-element.22) | copy-start | bytes 16900
  276.0 10.7 %copy-start.17 = (f32[1408]{0:T(1024)S(1)}, f32[1408]{0:T(1024)}, u32[]{:S(2)}) copy-start(f32[1408]{0:T(1024)} %get-tuple-element.23) | copy-start | bytes 16900
  276.0 10.7 %copy-start.18 = (f32[1408]{0:T(1024)S(1)}, f32[1408]{0:T(1024)}, u32[]{:S(2)}) copy-start(f32[1408]{0:T(1024)} %get-tuple-element.24) | copy-start | bytes 16900
  276.0 10.7 %copy-start.19 = (f32[1408]{0:T(1024)S(1)}, f32[1408]{0:T(1024)}, u32[]{:S(2)}) copy-start(f32[1408]{0:T(1024)} %get-tuple-element.44) | copy-start | bytes 16900
  276.0 10.7 %copy-start.20 = (f32[1408]{0:T(1024)S(1)}, f32[1408]{0:T(1024)}, u32[]{:S(2)}) copy-start(f32[1408]{0:T(1024)} %get-tuple-element.45) | copy-start | bytes 16900
  276.0 10.7 %copy-start.21 = (f32[1408]{0:T(1024)S(1)}, f32[1408]{0:T(1024)}, u32[]{:S(2)}) copy-start(f32[1408]{0:T(1024)} %get-tuple-element.46) | copy-start | bytes 16900
  276.0 10.7 %copy-start.8 = (f32[1024,1408]{1,0:T(8,128)S(1)}, f32[1024,1408]{1,0:T(8,128)}, u32[]{:S(2)}) copy-start(f32[1024,1408]{1,0:T(8,128)} %convolution_multiply_fusion) | copy-start | bytes 17301508
  292.0 3.3 copy-start.12
  292.0 3.3 copy-start.24
  295.3 1.8 copy-start.11
  295.3 1.8 copy-start.25
  297.2 1.8 copy-start.26
  300.8 47.1 %copy-start.1 = (f32[512,1408]{1,0:T(8,128)S(1)}, f32[512,1408]{1,0:T(8,128)}, u32[]{:S(2)}) copy-start(f32[512,1408]{1,0:T(8,128)} %param.34) | copy-start | bytes 8650756
Sparse Core Ops, SparseCore 0:
  9.6 112.6 all-gather.1
  303.3 41.7 reduce-scatter.1

commit v2 on v1

--- a/solution.py
+++ b/solution.py
@@ -15,17 +15,6 @@
 
 def expand_scale(gathered):
     return gathered.T.reshape(-1)
-
-
-def causal_mix(values, filter_taps, seq_len):
-    columns = values.shape[-1]
-    grouped = values.reshape(-1, seq_len, columns)
-    tap_count = filter_taps.shape[0]
-    padded = jnp.pad(grouped, ((0, 0), (tap_count - 1, 0), (0, 0)))
-    totals = padded[:, 0:seq_len] * filter_taps[0]
-    for k in range(1, tap_count):
-        totals = totals + padded[:, k : k + seq_len] * filter_taps[k]
-    return totals.reshape(-1, columns)
 
 
 def mixer_kernel(branch_ref, gelu_ref, bscale_ref, gscale_ref, taps_ref, rg_ref, ig_ref, sp_ref, out_ref):
@@ -63,26 +52,30 @@
     return jnp.einsum("gpab,pq->gpaqb", grouped, eye).reshape(count // per, per * width, per * width)
 
 
-def mixer(branch, gelu_in, bscale, gscale, taps, recur_gate, input_gate, softplus):
+def mixer(branch, gelu_in, flat, branch_start, gelu_start, taps, recur_gate, input_gate, softplus):
     rows, channels = branch.shape
     lanes = min(channels, 128)
     per = lanes // recur_gate.shape[1]
     rg, ig = block_diagonal(recur_gate, per), block_diagonal(input_gate, per)
     tile = pl.BlockSpec((SEQ_LEN, lanes), lambda s, c: (s, c))
     row = pl.BlockSpec((1, lanes), lambda s, c: (0, c))
+    bscale, boff = aligned(flat, branch_start, channels)
+    gscale, goff = aligned(flat, gelu_start, channels)
     gate = pl.BlockSpec((None, lanes, lanes), lambda s, c: (c, 0, 0))
     return pl.pallas_call(
         mixer_kernel,
         grid=(rows // SEQ_LEN, channels // lanes),
         out_shape=jax.ShapeDtypeStruct((rows, channels), jnp.bfloat16),
         in_specs=[
-            tile, tile, row, row,
+            tile, tile,
+            pl.BlockSpec((1, lanes), lambda s, c: (0, c + boff)),
+            pl.BlockSpec((1, lanes), lambda s, c: (0, c + goff)),
             pl.BlockSpec((taps.shape[0], lanes), lambda s, c: (0, c)),
             gate, gate, row,
         ],
         out_specs=tile,
         cost_estimate=pl.CostEstimate(flops=10**8, bytes_accessed=10 * rows * channels, transcendentals=rows * channels * 6),
-    )(branch, gelu_in, bscale[None], gscale[None], taps, rg, ig, softplus[None])
+    )(branch, gelu_in, bscale, gscale, taps, rg, ig, softplus[None])
 
 
 class Across:
@@ -247,10 +240,13 @@
     lax.fori_loop(0, rows // step, body, 0)
 
 
-def first_kernel(tp, fs, tokens, gain, mixer_src, scale_src, normed, mixers, scales, *scratch):
+def first_kernel(
+    tp, fs, tokens, gain, mixer_src, scale_src, gate_src, normed, mixers, scales, gate_out, *scratch
+):
     across = Across(tp, tokens, *scratch[:7])
     along = Along(fs, mixer_src, mixers, *scratch[7:9])
-    scale_sems, scale_local = scratch[9:]
+    scale_sems, scale_local = scratch[9:11]
+    gate = Along(fs, gate_src, gate_out, *scratch[11:13])
     greet(tp, fs)
     z = lax.axis_index("fs")
     along.start()
@@ -266,15 +262,20 @@
             recv_sem=scale_sems.at[1, d - 1], device_id={"fs": lax.rem(z + d, fs)},
             device_id_type=MESH))
         small[-1].start()
+    gate.start()
     for k in range(CHUNKS):
         across.forward(k)
         if k + 1 < fs:
             along.pump(k + 1)
     for s in range(CHUNKS + 1, fs):
         along.pump(s)
+    gate.pump(1)
     across.finish()
     norm_rows(tp, across.held, gain, normed)
     own.wait()
+    for s in range(2, fs):
+        gate.pump(s)
+    gate.finish()
     for copy in small:
         copy.wait()
     along.finish()
@@ -283,7 +284,7 @@
 ANY = pl.BlockSpec(memory_space=pl.ANY)
 
 
-def first(tp, fs, tokens, gain, mixer_src, scale_src):
+def first(tp, fs, tokens, gain, mixer_src, scale_src, gate_src):
     rows, columns = tokens.shape
     return pl.pallas_call(
         functools.partial(first_kernel, tp, fs),
@@ -291,15 +292,16 @@
             jax.ShapeDtypeStruct((rows, columns * tp), jnp.bfloat16),
             jax.ShapeDtypeStruct((fs,) + mixer_src.shape, jnp.bfloat16),
             jax.ShapeDtypeStruct((fs,) + scale_src.shape, jnp.float32),
+            jax.ShapeDtypeStruct((fs,) + gate_src.shape, jnp.bfloat16),
         ),
-        in_specs=[VMEM] * 4, out_specs=(VMEM, ANY, VMEM),
+        in_specs=[VMEM] * 5, out_specs=(VMEM, ANY, VMEM, ANY),
         scratch_shapes=across_scratch(tp, rows, columns) + along_scratch(fs) + [
-            pltpu.SemaphoreType.DMA((2, fs - 1)), pltpu.SemaphoreType.DMA],
+            pltpu.SemaphoreType.DMA((2, fs - 1)), pltpu.SemaphoreType.DMA] + along_scratch(fs),
         compiler_params=pltpu.CompilerParams(
             collective_id=0, has_side_effects=True, vmem_limit_bytes=40 * 2**20),
         cost_estimate=pl.CostEstimate(flops=10**7, bytes_accessed=60 * 2**20, transcendentals=0),
         name="first",
-    )(tokens, gain[None], mixer_src, scale_src)
+    )(tokens, gain[None], mixer_src, scale_src, gate_src)
 
 
 def second_kernel(
@@ -371,6 +373,155 @@
     )(state, weight, scale[None], tokens, gain[None], val_src, down_src)
 
 
+def last_kernel(
+    tp, left, down, scale, hidden, out, terms, near, pairs, far, kept,
+    near_send, near_recv, far_send, far_recv,
+):
+    me = lax.axis_index("tp")
+    core, chip, chips = lax.rem(me, 2), me // 2, tp // 2
+    partner = me + 1 - 2 * core
+    others = [lax.rem(chip + d, chips) for d in range(chips)]
+    barrier = pltpu.get_barrier_semaphore()
+    for device in [partner] + [c * 2 + core for c in others[1:]]:
+        pl.semaphore_signal(barrier, inc=1, device_id={"tp": device}, device_id_type=MESH)
+    pl.semaphore_wait(barrier, chips)
+    rows = left.shape[0] // CHUNKS
+    per = down.shape[0] // tp
+    piece = down.shape[2]
+
+    def term(k, block):
+        values = left[k * rows : (k + 1) * rows, :]
+        cols = [
+            jnp.dot(values, down[block * per + j], preferred_element_type=jnp.float32)
+            for j in range(per)]
+        whole = cols[0] if per == 1 else jnp.concatenate(cols, axis=1)
+        return (whole * scale[block]).astype(jnp.bfloat16)
+
+    def to_partner(k, c):
+        return pltpu.make_async_remote_copy(
+            src_ref=terms.at[k, 0, c], dst_ref=near.at[k, c], send_sem=near_send.at[k, c],
+            recv_sem=near_recv.at[k, c], device_id={"tp": partner}, device_id_type=MESH)
+
+    def to_chip(k, d):
+        return pltpu.make_async_remote_copy(
+            src_ref=pairs.at[k, d - 1], dst_ref=far.at[k, d - 1], send_sem=far_send.at[k, d - 1],
+            recv_sem=far_recv.at[k, d - 1], device_id={"tp": others[d] * 2 + core},
+            device_id_type=MESH)
+
+    def join(k):
+        for d in list(range(1, chips)) + [0]:
+            c = others[d]
+            to_partner(k, c).wait_recv()
+            total = terms[k, 1, c].astype(jnp.float32) + near[k, c].astype(jnp.float32)
+            if d:
+                pairs[k, d - 1] = total.astype(jnp.bfloat16)
+                to_chip(k, d).start()
+            else:
+                kept[k] = total
+
+    def close(k):
+        total = kept[k]
+        for d in range(1, chips):
+            to_chip(k, d).wait_recv()
+            total = total + far[k, d - 1].astype(jnp.float32)
+        part = slice(k * rows, (k + 1) * rows)
+        out[part, :] = (hidden[part, :].astype(jnp.float32) + total).astype(jnp.bfloat16)
+
+    for k in range(CHUNKS):
+        for d in list(range(1, chips)) + [0]:
+            c = others[d]
+            terms[k, 0, c] = term(k, c * 2 + 1 - core)
+            to_partner(k, c).start()
+        for d in list(range(1, chips)) + [0]:
+            c = others[d]
+            terms[k, 1, c] = term(k, c * 2 + core)
+        join(k)
+    for k in range(CHUNKS):
+        close(k)
+    for k in range(CHUNKS):
+        for c in others:
+            to_partner(k, c).wait_send()
+        for d in range(1, chips):
+            to_chip(k, d).wait_send()
+
+
+def last(tp, left, down, scale, hidden):
+    rows, width = hidden.shape
+    chips, part = tp // 2, rows // CHUNKS
+    return pl.pallas_call(
+        functools.partial(last_kernel, tp),
+        out_shape=jax.ShapeDtypeStruct(hidden.shape, jnp.bfloat16),
+        in_specs=[VMEM] * 4, out_specs=VMEM,
+        scratch_shapes=[
+            pltpu.VMEM((CHUNKS, 2, chips, part, width), jnp.bfloat16),
+            pltpu.VMEM((CHUNKS, chips, part, width), jnp.bfloat16),
+            pltpu.VMEM((CHUNKS, chips - 1, part, width), jnp.bfloat16),
+            pltpu.VMEM((CHUNKS, chips - 1, part, width), jnp.bfloat16),
+            pltpu.VMEM((CHUNKS, part, width), jnp.float32),
+            pltpu.SemaphoreType.DMA((CHUNKS, chips)), pltpu.SemaphoreType.DMA((CHUNKS, chips)),
+            pltpu.SemaphoreType.DMA((CHUNKS, chips - 1)),
+            pltpu.SemaphoreType.DMA((CHUNKS, chips - 1)),
+        ],
+        compiler_params=pltpu.CompilerParams(
+            collective_id=2, has_side_effects=True, vmem_limit_bytes=48 * 2**20),
+        cost_estimate=pl.CostEstimate(flops=10**10, bytes_accessed=60 * 2**20, transcendentals=0),
+        name="last",
+    )(left, down, scale.reshape(tp, 1, width), hidden)
+
+
+def aligned(flat, start, size):
+    if start % 128 == 0:
+        return flat, start // 128
+    return flat[:, start : start + size], 0
+
+
+def up_kernel(left_ref, gate_ref, val_ref, gscale_ref, vscale_ref, gtaps_ref, vtaps_ref, out_ref):
+    lanes = gate_ref.shape[1]
+    weight = jnp.concatenate([gate_ref[...], val_ref[...]], axis=1)
+
+    def mixed(values, scale_ref, taps_ref):
+        values = values * scale_ref[...]
+        position = lax.broadcasted_iota(jnp.int32, values.shape, 0)
+        taps = taps_ref.shape[0]
+        total = values * taps_ref[taps - 1 : taps, :]
+        for shift in range(1, taps):
+            delayed = jnp.where(position >= shift, pltpu.roll(values, shift, 0), 0.0)
+            total = total + delayed * taps_ref[taps - 1 - shift : taps - shift, :]
+        return total
+
+    for s in range(left_ref.shape[0] // SEQ_LEN):
+        part = slice(s * SEQ_LEN, (s + 1) * SEQ_LEN)
+        both = jnp.dot(left_ref[part, :], weight, preferred_element_type=jnp.float32)
+        gate = mixed(both[:, :lanes], gscale_ref, gtaps_ref)
+        value = mixed(both[:, lanes:], vscale_ref, vtaps_ref)
+        out_ref[part, :] = (jax.nn.silu(gate) * value).astype(jnp.bfloat16)
+
+
+def up(left, gate, val, flat, gate_start, val_start, gate_taps, val_taps):
+    rows, depth = left.shape
+    columns = gate.shape[1]
+    lanes = 128
+    gscale, goff = aligned(flat, gate_start, columns)
+    vscale, voff = aligned(flat, val_start, columns)
+    tile = pl.BlockSpec((depth, lanes), lambda c: (0, c))
+    tap = pl.BlockSpec((gate_taps.shape[0], lanes), lambda c: (0, c))
+    return pl.pallas_call(
+        up_kernel,
+        grid=(pl.cdiv(columns, lanes),),
+        out_shape=jax.ShapeDtypeStruct((rows, columns), jnp.bfloat16),
+        in_specs=[
+            pl.BlockSpec((rows, depth), lambda c: (0, 0)), tile, tile,
+            pl.BlockSpec((1, lanes), lambda c: (0, c + goff)),
+            pl.BlockSpec((1, lanes), lambda c: (0, c + voff)), tap, tap,
+        ],
+        out_specs=pl.BlockSpec((rows, lanes), lambda c: (0, c)),
+        compiler_params=pltpu.CompilerParams(vmem_limit_bytes=32 * 2**20),
+        cost_estimate=pl.CostEstimate(
+            flops=4 * rows * depth * columns, bytes_accessed=20 * 2**20, transcendentals=rows * columns),
+        name="up",
+    )(left, gate, val, gscale, vscale, gate_taps, val_taps)
+
+
 def half_rows(weight):
     count = lax.axis_size("grp")
     rows = weight.shape[0] // count
@@ -394,49 +545,41 @@
 ):
     tp = lax.axis_size("tp")
     fs = lax.axis_size("fs")
-    gate_full = whole_rows(upgate_weight)
     scale_list = (branch_scale, gelu_scale, out_scale, upgate_scale, upval_scale, down_scale)
     lru = branch_weight.shape[1]
     depth = branch_weight.shape[0] // 2
     mixer_src = jnp.concatenate(
         [halves(branch_weight), halves(gelu_weight), halves(out_weight.reshape(-1, lru))], axis=1)
-    normed, mixers, packed = first(
-        tp, fs, tokens, mixer_gain, mixer_src, jnp.concatenate(scale_list, axis=1))
-    packed = packed[:, 0]
-    scales, start = [], 0
+    normed, mixers, packed, gate_full = first(
+        tp, fs, tokens, mixer_gain, mixer_src, jnp.concatenate(scale_list, axis=1),
+        halves(upgate_weight))
+    gate_full = gate_full.reshape(-1, upgate_weight.shape[1])
+    flat = expand_scale(packed[:, 0])[None]
+    starts = [0]
     for piece in scale_list:
-        scales.append(expand_scale(packed[:, start : start + piece.shape[1]]))
-        start += piece.shape[1]
+        starts.append(starts[-1] + piece.shape[1] * fs)
     rows_branch = mixers[:, :, :depth].reshape(-1, lru)
     rows_gelu = mixers[:, :, depth : 2 * depth].reshape(-1, lru)
     out_blocks = mixers[:, :, 2 * depth :].reshape((fs,) + out_weight.shape)
     branch = jnp.dot(normed, rows_branch, preferred_element_type=jnp.float32)
     gelu_in = jnp.dot(normed, rows_gelu, preferred_element_type=jnp.float32)
     gated_state = mixer(
-        branch, gelu_in, scales[0], scales[1], branch_taps, recur_gate, input_gate,
+        branch, gelu_in, flat, starts[0], starts[1], branch_taps, recur_gate, input_gate,
         jax.nn.softplus(-decay_param))
     row_block = jnp.transpose(out_blocks, (1, 0, 2)).reshape(out_weight.shape[0], -1)
     own_columns = lax.all_to_all(row_block, "tp", split_axis=1, concat_axis=0, tiled=True)
     width = tokens.shape[1]
-    own_scales = lax.dynamic_slice_in_dim(scales[2], lax.axis_index("tp") * width, width, 0)
+    own_scales = lax.dynamic_slice_in_dim(
+        flat[0], starts[2] + lax.axis_index("tp") * width, width, 0)
     hidden_state, normed_ffn, value_full, down_blocks = second(
         tp, fs, gated_state, own_columns, own_scales, tokens, ffn_gain,
         halves(upval_weight), halves(down_weight))
     value_full = value_full.reshape(-1, upval_weight.shape[1])
     down_blocks = down_blocks.reshape((fs,) + down_weight.shape)
-    up_gate = jnp.dot(normed_ffn, gate_full, preferred_element_type=jnp.float32)
-    up_val = jnp.dot(normed_ffn, value_full, preferred_element_type=jnp.float32)
-    conv_gate = causal_mix(up_gate * scales[3], upgate_taps, SEQ_LEN)
-    conv_val = causal_mix(up_val * scales[4], upval_taps, SEQ_LEN)
-    ffn_hidden = (jax.nn.silu(conv_gate) * conv_val).astype(jnp.bfloat16)
-    piece = down_blocks.shape[2]
-    terms = []
-    for f in range(down_blocks.shape[0]):
-        term = jnp.dot(ffn_hidden, down_blocks[f], preferred_element_type=jnp.float32)
-        terms.append((term * scales[5][f * piece : (f + 1) * piece]).astype(jnp.bfloat16))
-    ffn_terms = jnp.concatenate(terms, axis=1)
-    ffn_sum = lax.psum_scatter(ffn_terms, "tp", scatter_dimension=1, tiled=True).astype(jnp.float32)
-    return (hidden_state.astype(jnp.float32) + ffn_sum).astype(jnp.bfloat16)
+    ffn_hidden = up(
+        normed_ffn, gate_full, value_full, flat, starts[3], starts[4], upgate_taps, upval_taps)
+    down_scales = flat[0, starts[5] : starts[5] + down_scale.shape[1] * fs]
+    return last(tp, ffn_hidden, down_blocks, down_scales, hidden_state)
 
 
 def solution(mesh):

time: 356 us -> 321 us (0.902)
  Pallas kernels: 203 us -> 279 us
  waiting for transfers between devices: 42 us -> 0.01 us
  matrix products: 37.3 us -> 7.15 us
  local copies, waits for them, and re-layouts: 39.1 us -> 21.2 us
  between operations: 13.9 us -> 0.27 us
  other arithmetic: 15.8 us -> 9.69 us
    pallas_call x0 -> x2, Pallas kernels: none -> 50.6 us  [the longest x1 30.5 us: last(): pl.pallas_call(functools.partial(last_kernel, tp), out_shape=jax.ShapeDty...]
    reduce_scatter x1 -> x0, waiting for transfers between devices: 42 us -> none  [per_device(): lax.psum_scatter(ffn_terms, 'tp', scatter_dimension=1, tiled=True)]
    dot_general x6 -> x0, matrix products: 27.6 us -> none  [the longest x1 10.6 us: per_device(): up_gate = jnp.dot(normed_ffn, gate_full, preferred_element_type=jnp.float32)]
    pallas_call x1, Pallas kernels: 77.9 us -> 104 us  [first(): pl.pallas_call(functools.partial(first_kernel, tp, fs), out_shape=(jax.Sh...]
    slice x7 -> x1, local copies, waits for them, and re-layouts: 12.9 us -> 1.29 us  [per_device(): down_scales = flat[0, starts[5]:starts[5] + down_scale.shape[1] * fs]]
    mul x6 -> x0, local copies, waits for them, and re-layouts: 8.8 us -> none  [the longest x4 5.5 us: per_device(): term * scales[5][f * piece:(f + 1) * piece]]
    convert_element_type x2 -> x0, other arithmetic: 8.1 us -> none  [the longest x1 5.31 us: per_device(): ffn_hidden = (jax.nn.silu(conv_gate) * conv_val).astype(jnp.bfloat16)]
    convert_element_type x5 -> x6, other arithmetic: 3.73 us -> 8.72 us  [halves(): weight.astype(jnp.bfloat16)]
  transfers between devices with their start and end apart: 3 -> 1, of which waited for: 1 -> 0; matrix products, arithmetic and copies ran while one was open for 15% -> 6% of each run, Pallas kernels for 57% -> 2%
where the time goes in v2:
time: 321 us; the launch traced here: 320 us
  Pallas kernels  279 us (87%)
  local copies, waits for them, and re-layouts  21.2 us (7%)
  other arithmetic  9.69 us (3%)
  matrix products  7.15 us (2%)
  starting transfers between devices  3.65 us (1%)
    pallas_call x1, Pallas kernels, second(): pl.pallas_call(functools.partial(second_kernel, tp, fs), out_shape=(jax.S...  118 us
    pallas_call x1, Pallas kernels, first(): pl.pallas_call(functools.partial(first_kernel, tp, fs), out_shape=(jax.Sh...  104 us
    pallas_call x1, Pallas kernels, last(): pl.pallas_call(functools.partial(last_kernel, tp), out_shape=jax.ShapeDty...  30.5 us
    pallas_call x1, Pallas kernels, up(): pl.pallas_call(up_kernel, grid=(pl.cdiv(columns, lanes),), out_shape=jax....  20.1 us
    unnamed x46, local copies, waits for them, and re-layouts  10.9 us
    convert_element_type x6, other arithmetic, halves(): weight.astype(jnp.bfloat16)  8.72 us
  transfers between devices with their start and end apart: 1, of which 0 were waited for; matrix products, arithmetic and copies ran while one was open for 6% of the time, Pallas kernels for 2%

profile of v2, /device:TPU:0, one launch (start us, length us, event | category | flops | bytes accessed | tf_op | source)
XLA Modules:
  0.0 320.4 jit_solution(1168597754755462963)
XLA Ops:
  0.0 1.1 convert_element_type.26
  1.1 0.1 convert_element_type.27
  1.2 1.1 convert_element_type.24
  2.2 1.1 convert_element_type.25
  3.3 0.0 copy-start.19
  3.3 0.0 copy-start.20
  3.3 0.0 copy-start
  3.4 0.0 copy-start.5
  3.4 2.1 convert_element_type.28
  5.4 0.1 pad_maximum_fusion.mixer_src
  5.5 0.0 copy-done.19
  5.5 0.0 copy-done.20
  5.5 0.8 concatenate.7.scale_src
  6.3 0.0 copy-done
  6.3 0.0 copy-done.5
  6.4 104.3 %first.1 = (bf16[1024,2048]{1,0:T(8,128)(2,1)S(1)}, bf16[4,2,768,256]{3,2,1,0:T(8,128)(2,1)S(1)}, f32[4,1,1856]{2,1,0:T(1,128)S(1)}, bf16[4,2,256,1408]{3,2,1,0:T(8,128)(2,1)}) custom-call(bf16[1024,512]{1,0:T(8,128)(2,1)S(1)} %copy-done, f32[1,2048]{1,0:T(1,128)S(1)} %bitcast.44, bf16[2,768,256]{2,1,0:T(8,128)(2,1)S(1)} %pad_maximum_fusion.mixer_src, ...), custom_call_target="tpu_custom_call" | custom-call | flops 10000000 | bytes 62914560 | tf_op jit(solution)/shard_map/first/pallas_call | solution.py:289
  110.6 0.0 copy-start.3
  110.6 0.0 copy-start.10
  110.7 1.9 fusion
  112.5 0.0 copy-done.3
  112.5 0.8 copy-done.10
  113.3 0.0 copy-start.4
  113.3 0.0 copy-start.17
  113.3 0.0 copy-start.18
  113.3 1.2 reshape.69
  114.5 0.0 copy-start.21
  114.5 3.6 %all-to-all-start = ((bf16[256,4,512]{2,0,1:T(8,128)(2,1)}), bf16[256,4,512]{2,0,1:T(8,128)(2,1)S(1)}, u32[]{:S(2)}, u32[]{:S(2)}) async-start(bf16[256,4,512]{2,0,1:T(8,128)(2,1)} %bitcast.14), calls=%async_computation | async-start | bytes 2097152 | tf_op jit(solution)/shard_map/all_to_all | solution.py:570
  118.2 0.0 copy-done.4
  118.2 0.3 copy.23
  118.5 1.3 broadcast_in_dim_reshape.3.bscale_ref.gscale_ref.vscale_ref
  119.8 1.2 squeeze_broadcast_in_dim_reshape.3
  121.0 0.0 copy-done.17
  121.0 0.0 copy-done.18
  121.0 0.3 multiply_bitcast_fusion
  121.3 0.8 reshape.65.rg_ref
  122.0 0.7 reshape.68.ig_ref
  122.8 0.0 copy-done.21
  122.8 0.6 compare_select_fusion
  123.4 2.1 convert_element_type.29
  125.5 0.6 copy-done.15
  126.1 1.3 convert_element_type.30
  127.4 1.3 slice.16
  128.7 0.8 dynamic_slice.3
  129.5 4.9 %fusion.2.gelu_ref = f32[1024,256]{1,0:T(8,128)} fusion(bf16[1024,2048]{1,0:T(8,128)(2,1)} %copy-done.10, bf16[2048,256]{1,0:T(8,128)(2,1)} %bitcast.53), kind=kOutput, calls=%fused_computation.8 | convolution fusion | flops 1073741824 | bytes 6291456 | tf_op jit(solution)/shard_map/dot_general | solution.py:565
  134.4 0.0 copy-done.11
  134.4 0.0 copy-done.16
  134.4 2.2 fusion.1.branch_ref
  136.6 5.5 %shard_map.199.state = bf16[1024,256]{1,0:T(8,128)(2,1)} custom-call(f32[1024,256]{1,0:T(8,128)} %fusion.1.branch_ref, f32[1024,256]{1,0:T(8,128)} %fusion.2.gelu_ref, f32[1,7424]{1,0:T(1,128)} %broadcast_in_dim_reshape.3.bscale_ref.gscale_ref.vscale_ref, f32[1,7424]{1,0:T(1,128)} %broadcast_in_dim_reshape.3.bscale_ref.gscale_ref.vscale_ref, ...), custom_call_target="tpu_custom_call" | custom-call | flops 100000000 | bytes 2621440 | tf_op jit(solution)/shard_map/pallas_call | solution.py:65
  142.1 0.0 all-to-all-done
  142.1 0.0 copy-done.6
  142.1 0.0 copy-start.1
  142.2 1.0 copy-done.1
  143.2 118.2 %second.1 = (bf16[1024,512]{1,0:T(8,128)(2,1)S(1)}, bf16[1024,2048]{1,0:T(8,128)(2,1)}, bf16[4,2,256,1408]{3,2,1,0:T(8,128)(2,1)}, bf16[4,2,704,512]{3,2,1,0:T(8,128)(2,1)}) custom-call(bf16[1024,256]{1,0:T(8,128)(2,1)S(1)} %copy-done.1, bf16[1024,512]{1,0:T(8,128)(2,1)S(1)} %bitcast.42, f32[1,512]{1,0:T(1,128)S(1)} %bitcast.43, ...), custom_call_target="tpu_custom_call" | custom-call | flops 1000000000 | bytes 188743680 | tf_op jit(solution)/shard_map/second/pallas_call | solution.py:358
  261.4 0.0 copy-done.2
  261.4 0.0 copy-done.13
  261.4 0.0 copy-done.14
  261.4 0.0 copy-start.8
  261.4 2.6 copy-done.8
  264.1 2.6 copy-done.9
  266.7 2.2 copy-done.12
  268.9 20.1 %up.1.left = bf16[1024,1408]{1,0:T(8,128)(2,1)S(1)} custom-call(bf16[1024,2048]{1,0:T(8,128)(2,1)S(1)} %copy-done.12, bf16[2048,1408]{1,0:T(8,128)(2,1)S(1)} %bitcast.47, bf16[2048,1408]{1,0:T(8,128)(2,1)S(1)} %bitcast.48, f32[1,7424]{1,0:T(1,128)S(1)} %copy-done.2, f32[1,7424]{1,0:T(1,128)S(1)} %copy-done.2, f32[3,1408]{1,0:T(4,128)S(1)} %copy-done.13, ...), custom_call_target="tpu_custom_call" | custom-call | flops 11811160064 | bytes 20971520 | tf_op jit(solution)/shard_map/up/pallas_call | solution.py:508
  289.0 0.0 copy-done.7
  289.0 30.5 %last.1 = bf16[1024,512]{1,0:T(8,128)(2,1)S(1)} custom-call(bf16[1024,1408]{1,0:T(8,128)(2,1)S(1)} %up.1.left, bf16[4,1408,512]{2,1,0:T(8,128)(2,1)} %bitcast.58, f32[4,1,512]{2,1,0:T(1,128)S(1)} %bitcast.46, bf16[1024,512]{1,0:T(8,128)(2,1)S(1)} %get-tuple-element.20.hidden), custom_call_target="tpu_custom_call" | custom-call | flops 10000000000 | bytes 62914560 | tf_op jit(solution)/shard_map/last/pallas_call | solution.py:451
  319.5 1.0 copy.29
  (12 shorter events, 0.0 us)
Async XLA Ops:
  3.3 2.2 copy-start.19
  3.3 2.2 copy-start.20
  3.3 3.0 copy-start
  3.4 3.0 copy-start.5
  110.6 1.9 copy-start.3
  110.6 2.7 copy-start.10
  113.3 4.8 %copy-start.4 = (f32[4,1,1856]{2,1,0:T(1,128)S(1)}, f32[4,1,1856]{2,1,0:T(1,128)}, u32[]{:S(2)}) copy-start(f32[4,1,1856]{2,1,0:T(1,128)} %copy-done.3) | copy-start | bytes 89092
  113.3 7.7 %copy-start.17 = (bf16[4,64,64]{2,1,0:T(8,128)(2,1)S(1)}, bf16[4,64,64]{2,1,0:T(8,128)(2,1)}, u32[]{:S(2)}) copy-start(bf16[4,64,64]{2,1,0:T(8,128)(2,1)} %param.29) | copy-start | bytes 98308
  113.3 7.7 %copy-start.18 = (bf16[4,64,64]{2,1,0:T(8,128)(2,1)S(1)}, bf16[4,64,64]{2,1,0:T(8,128)(2,1)}, u32[]{:S(2)}) copy-start(bf16[4,64,64]{2,1,0:T(8,128)(2,1)} %param.28) | copy-start | bytes 98308
  114.5 8.3 %copy-start.21 = (f32[256]{0:T(256)S(1)}, f32[256]{0:T(256)}, u32[]{:S(2)}) copy-start(f32[256]{0:T(256)} %param.30) | copy-start | bytes 3076
  114.5 27.6 %all-to-all-start = ((bf16[256,4,512]{2,0,1:T(8,128)(2,1)}), bf16[256,4,512]{2,0,1:T(8,128)(2,1)S(1)}, u32[]{:S(2)}, u32[]{:S(2)}) async-start(bf16[256,4,512]{2,0,1:T(8,128)(2,1)} %bitcast.14), calls=%async_computation | async-start | bytes 2097152 | tf_op jit(solution)/shard_map/all_to_all | solution.py:570
  123.4 2.7 copy-start.15
  129.5 4.9 %copy-start.11 = (bf16[1024,2048]{1,0:T(8,128)(2,1)S(1)}, bf16[1024,2048]{1,0:T(8,128)(2,1)}, u32[]{:S(2)}) copy-start(bf16[1024,2048]{1,0:T(8,128)(2,1)} %copy-done.10) | copy-start | bytes 12582916
  129.5 4.9 %copy-start.16 = (bf16[4,2,256,256]{3,2,1,0:T(8,128)(2,1)S(1)}, bf16[4,2,256,256]{3,2,1,0:T(8,128)(2,1)}, u32[]{:S(2)}) copy-start(bf16[4,2,256,256]{3,2,1,0:T(8,128)(2,1)} %get-tuple-element.23) | copy-start | bytes 3145732
  134.4 7.7 %copy-start.6 = (f32[2048]{0:T(1024)S(1)}, f32[2048]{0:T(1024)}, u32[]{:S(2)}) copy-start(f32[2048]{0:T(1024)} %param.33) | copy-start | bytes 24580
  142.1 1.0 copy-start.1
  143.2 118.2 %copy-start.2 = (f32[1,7424]{1,0:T(1,128)S(1)}, f32[1,7424]{1,0:T(1,128)}, u32[]{:S(2)}) copy-start(f32[1,7424]{1,0:T(1,128)} %broadcast_in_dim_reshape.3.bscale_ref.gscale_ref.vscale_ref) | copy-start | bytes 89092
  143.2 118.2 %copy-start.13 = (f32[3,1408]{1,0:T(4,128)S(1)}, f32[3,1408]{1,0:T(4,128)}, u32[]{:S(2)}) copy-start(f32[3,1408]{1,0:T(4,128)} %gtaps_ref.1) | copy-start | bytes 50692
  143.2 118.2 %copy-start.14 = (f32[3,1408]{1,0:T(4,128)S(1)}, f32[3,1408]{1,0:T(4,128)}, u32[]{:S(2)}) copy-start(f32[3,1408]{1,0:T(4,128)} %vtaps_ref.1) | copy-start | bytes 50692
  261.4 2.6 copy-start.8
  264.1 2.6 copy-start.9
  266.7 2.2 copy-start.12
  268.9 20.1 %copy-start.7 = (f32[1,2048]{1,0:T(1,128)S(1)}, f32[1,2048]{1,0:T(1,128)}, u32[]{:S(2)}) copy-start(f32[1,2048]{1,0:T(1,128)} %slice.16) | copy-start | bytes 24580
